TPU v7x, 32 devices: a whole 2x2x4 slice. The times are simulated.
32 devices in a mesh: grp: 2 (over x), tp: 16 (over z, y, core).
Axes of the slice: x: 2, y: 2, z: 4, core: 2. Of those that a mesh axis runs over, the one named last changes fastest.
Arguments:
- tokens: bfloat16 [3072, 2048], P('grp', 'tp'), parts along dimension 0, may hold values from -6 to 6
- lengths: int32 [192], P('grp'), parts along dimension 0, may hold values from 1 to 16, 960 in all
- gain_first: float32 [2048], replicated, may hold values from 0.1 to 1.9
- query_first: bfloat16 [2048, 1024], P(None, 'tp'), may hold values from -0.125 to 0.125
- key_first: bfloat16 [2048, 1024], P(None, 'tp'), may hold values from -0.125 to 0.125
- value_first: bfloat16 [2048, 2048], P(None, 'tp'), may hold values from -0.125 to 0.125
- gate_first: bfloat16 [2048, 2048], P(None, 'tp'), may hold values from -0.125 to 0.125
- out_first: bfloat16 [2048, 2048], P('tp'), may hold values from -0.1875 to 0.1875
- state_first: float32 [192, 16, 64, 128], P('grp', 'tp'), parts along dimension 0, may hold values from -0.9 to 0.9
- gain_second: float32 [2048], replicated, may hold values from 0.1 to 1.9
- query_second: bfloat16 [2048, 1024], P(None, 'tp'), may hold values from -0.125 to 0.125
- key_second: bfloat16 [2048, 1024], P(None, 'tp'), may hold values from -0.125 to 0.125
- value_second: bfloat16 [2048, 2048], P(None, 'tp'), may hold values from -0.125 to 0.125
- gate_second: bfloat16 [2048, 2048], P(None, 'tp'), may hold values from -0.125 to 0.125
- out_second: bfloat16 [2048, 2048], P('tp'), may hold values from -0.1875 to 0.1875
- state_second: float32 [192, 16, 64, 128], P('grp', 'tp'), parts along dimension 0, may hold values from -0.9 to 0.9
Outputs:
- mixed_out: bfloat16 [3072, 2048], P('grp', 'tp'), parts along dimension 0
- state_first_new: float32 [192, 16, 64, 128], P('grp', 'tp'), parts along dimension 0
- state_second_new: float32 [192, 16, 64, 128], P('grp', 'tp'), parts along dimension 0
There are 2 independent parts, one for each index of `grp`. A program takes and returns all parts, laid end to end along the dimension named above; an argument that names none is the same for every part. Nothing has to cross between parts.
All inputs are finite; a program needn't handle non-finite values.
Results may differ from a plain program's by a relative error of at most 0.025.
Values may be sent and summed in bfloat16 or wider, within the bound.
A program may use at most 128 MiB of HBM per device.

v0:
```python
import functools

import jax
import jax.numpy as jnp
from jax import lax
from jax.experimental import pallas as pl
from jax.experimental.pallas import tpu as pltpu
from jax.sharding import PartitionSpec as P

PAST_LEN = 16384
LIVE_TOTAL = 960

NORM_EPSILON = 1e-06
ROPE_BASE = 10000.0

MESH = pl.DeviceIdType.MESH
F32 = jnp.float32
BF16 = jnp.bfloat16


def decay_logs(head_count):
    head_total = lax.axis_size("tp") * head_count
    head_ids = (lax.axis_index("tp") * head_count + jnp.arange(head_count)).astype(F32)
    return jnp.log(1.0 - 2.0 ** (-1.5 - 6.0 * head_ids / (head_total - 1)))


def rope_tables(block_len, key_dim):
    half_dim = key_dim // 2
    inverse = ROPE_BASE ** (-jnp.arange(half_dim, dtype=F32) / half_dim)
    positions = PAST_LEN + jnp.arange(block_len, dtype=F32)
    angles = positions[:, None] * inverse[None, :]
    cosines, sines = jnp.cos(angles), jnp.sin(angles)
    cosines = jnp.concatenate([cosines, cosines], axis=1)
    sines = jnp.concatenate([-sines, sines], axis=1)
    scale = key_dim ** (-0.5)
    return jnp.concatenate([cosines, cosines * scale, sines, sines * scale], axis=1)


def retain(qkv, lengths, state_in):
    batch_size, head_count, key_dim, value_dim = state_in.shape
    block_len = qkv.shape[0] // batch_size
    log_gamma = decay_logs(head_count)
    queries = qkv[:, :key_dim].reshape(batch_size, block_len, 1, key_dim)
    key_rows = qkv[:, key_dim : 2 * key_dim].reshape(batch_size, block_len, 1, key_dim)
    values = qkv[:, 2 * key_dim :].reshape(batch_size, block_len, 1, value_dim)
    slot_ids = jnp.arange(block_len).astype(F32)
    live_count = lengths.astype(F32)
    active = (slot_ids[None, :] < live_count[:, None]).astype(F32)
    step_gap = slot_ids[:, None] - slot_ids[None, :]
    causal = (step_gap >= 0.0).astype(F32)
    within = jnp.exp(log_gamma[:, None, None] * jnp.maximum(step_gap, 0.0)[None]) * causal[None]
    scores = jnp.einsum("bihd,bjhd->bhij", queries, key_rows, preferred_element_type=F32)
    weights = (scores * within[None]).astype(BF16)
    inner_part = jnp.einsum("bhij,bjhe->bihe", weights, values, preferred_element_type=F32)
    carried = jnp.einsum(
        "bihd,bhde->bihe", queries.astype(F32), state_in, precision=lax.Precision.HIGHEST
    )
    carried = (
        carried * jnp.exp(log_gamma[None, None, :] * (slot_ids[None, :, None] + 1.0))[..., None]
    )
    retained = (inner_part + carried) * active[:, :, None, None]
    lead_gap = live_count[:, None] - 1.0 - slot_ids[None, :]
    key_weight = (
        jnp.exp(log_gamma[None, None, :] * jnp.maximum(lead_gap, 0.0)[:, :, None])
        * active[:, :, None]
    )
    added_state = jnp.einsum(
        "bjhd,bjhe->bhde",
        key_rows.astype(F32) * key_weight[..., None],
        values.astype(F32),
        precision=lax.Precision.HIGHEST,
    )
    new_state = (
        state_in * jnp.exp(log_gamma[None, :] * live_count[:, None])[:, :, None, None] + added_state
    )
    inv_rms = lax.rsqrt(jnp.mean(retained * retained, axis=-1, keepdims=True) + NORM_EPSILON)
    normed = (retained * inv_rms).astype(BF16)
    return normed.reshape(batch_size * block_len, value_dim), new_state


def retention_kernel(key_dim, block_len, *refs):
    decay, side_ref, row_ref, within_ref, qkv_ref, gate_ref, state_ref = refs[:7]
    h_ref, new_ref, total = refs[7:]
    i = pl.program_id(0)
    rows = qkv_ref.shape[0]
    both = 2 * key_dim
    size = side_ref.shape[0]
    side = side_ref[...]
    unit = within_ref.shape[0]
    group = unit // block_len

    slots = lax.broadcasted_iota(jnp.int32, (size, rows), 1)
    hot = jnp.where(slots == side[:, 0:1].astype(jnp.int32), 1.0, 0.0).astype(BF16)
    padded = jnp.dot(hot, qkv_ref[...], preferred_element_type=F32)
    wide = (unit, group * key_dim)
    own = lax.div(lax.broadcasted_iota(jnp.int32, wide, 0), block_len) == lax.div(
        lax.broadcasted_iota(jnp.int32, wide, 1), key_dim
    )
    front = lax.broadcasted_iota(jnp.int32, (unit, both), 1) < key_dim

    def per_sequence(doubled):
        spread = jnp.concatenate([doubled] * (group // 2), axis=1)
        return jnp.where(own, spread, 0.0).astype(BF16)

    def one(u):
        at = slice(u * unit, (u + 1) * unit)
        first = u * group
        qk, values = padded[at, :both], padded[at, both:].astype(BF16)
        turned = pltpu.roll(qk, key_dim, 1)
        queries, keys = jnp.where(front, qk, turned), jnp.where(front, turned, qk)
        scores = lax.dot_general(
            jnp.where(front, qk, 0.0).astype(BF16),
            keys.astype(BF16),
            (((1,), (1,)), ((), ())),
            preferred_element_type=F32,
        )
        weights = (scores * within_ref[...]).astype(BF16)
        retained = jnp.dot(weights, values, preferred_element_type=F32)
        state = state_ref[first : first + group].reshape(group * key_dim, state_ref.shape[-1])
        high = state.astype(BF16)
        low = (state - high.astype(F32)).astype(BF16)
        wide_q = per_sequence(queries)
        carried = jnp.dot(wide_q, high, preferred_element_type=F32)
        carried = carried + jnp.dot(wide_q, low, preferred_element_type=F32)
        retained = retained + carried * side[at, 1:2]
        inv = lax.rsqrt(jnp.mean(retained * retained, axis=-1, keepdims=True) + NORM_EPSILON)

        scaled = keys * side[at, 2:3]
        k_high = scaled.astype(BF16).astype(F32)
        added = None
        for piece in (k_high, scaled - k_high):
            term = lax.dot_general(
                per_sequence(piece), values, (((0,), (0,)), ((), ())), preferred_element_type=F32
            )
            added = term if added is None else added + term
        for b in range(group):
            new_ref[first + b] = (
                state_ref[first + b] * decay[i * (size // block_len) + first + b]
                + added[b * key_dim : (b + 1) * key_dim, :]
            )
        return (retained * inv).astype(BF16)

    normed = jnp.concatenate([one(u) for u in range(size // unit)], axis=0)
    places = lax.broadcasted_iota(jnp.int32, (rows, size), 0)
    back = jnp.where(places == row_ref[...], 1.0, 0.0).astype(BF16)
    part = jnp.dot(back, normed, preferred_element_type=F32)

    @pl.when(i == 0)
    def _():
        total[...] = part

    @pl.when(i > 0)
    def _():
        total[...] += part

    @pl.when(i == pl.num_programs(0) - 1)
    def _():
        h_ref[...] = (total[...] * gate_ref[...]).astype(BF16)


def retain_packed(decay, side, row, within, qkv, gate, state, block_len):
    batch_size, _, key_dim, value_dim = state.shape
    rows = qkv.shape[0]
    unit = within.shape[0]
    many = next(k for k in (3, 2, 1) if batch_size * block_len % (k * unit) == 0)
    size = many * unit
    group = size // block_len
    whole = lambda *shape: pl.BlockSpec(shape, lambda i: (0,) * len(shape))
    state_spec = pl.BlockSpec((group, key_dim, value_dim), lambda i: (i, 0, 0))
    h, new_state = pl.pallas_call(
        functools.partial(retention_kernel, key_dim, block_len),
        grid=(batch_size // group,),
        out_shape=[
            jax.ShapeDtypeStruct((rows, value_dim), BF16),
            jax.ShapeDtypeStruct((batch_size, key_dim, value_dim), F32),
        ],
        in_specs=[
            pl.BlockSpec(memory_space=pltpu.SMEM),
            pl.BlockSpec((size, side.shape[1]), lambda i: (i, 0)),
            pl.BlockSpec((1, size), lambda i: (0, i)),
            whole(unit, unit),
            whole(*qkv.shape),
            whole(*gate.shape),
            state_spec,
        ],
        out_specs=[whole(rows, value_dim), state_spec],
        scratch_shapes=[pltpu.VMEM((rows, value_dim), F32)],
        compiler_params=pltpu.CompilerParams(dimension_semantics=("arbitrary",)),
    )(decay, side, row, within, qkv, gate, state.reshape(batch_size, key_dim, value_dim))
    return h, new_state.reshape(state.shape)


class Ring:
    def __init__(self, n, rows, pieces):
        self.n, self.m = n, n // 2
        self.rows, self.pieces = rows, pieces
        self.size = rows // pieces
        me = lax.axis_index("tp")
        self.core = lax.rem(me, 2)
        chip = lax.div(me, 2)
        odd = lax.rem(chip, 2)
        half = lax.div(chip, 2)
        self.pos = (1 - odd) * half + odd * (self.m - 1 - half)
        self.me = me
        self.partner = chip * 2 + 1 - self.core
        self.right = self.device(self.pos + 1)
        self.left = self.device(self.pos - 1)

    def device(self, pos, other=False):
        m = self.m
        pos = lax.rem(pos + m, m)
        far = lax.div(pos, (m + 1) // 2)
        chip = (1 - far) * 2 * pos + far * (2 * (m - 1 - pos) + 1)
        return chip * 2 + (1 - self.core if other else self.core)

    def enter(self):
        barrier = pltpu.get_barrier_semaphore()
        for device in (self.left, self.right, self.partner):
            pl.semaphore_signal(barrier, inc=1, device_id={"tp": device}, device_id_type=MESH)
        pl.semaphore_wait(barrier, 3)

    def piece(self, j):
        return pl.ds(j * self.size, self.size)

    def clockwise(self, j):
        return j < self.pieces // 2

    def to(self, j):
        return self.right if self.clockwise(j) else self.left

    def back(self, j, steps):
        return self.pos - steps if self.clockwise(j) else self.pos + steps

    def order(self):
        half = self.pieces // 2
        return [j for pair in range(half) for j in (pair, pair + half)]


def remote(src, dst, send, recv, device):
    return pltpu.make_async_remote_copy(
        src_ref=src,
        dst_ref=dst,
        send_sem=send,
        recv_sem=recv,
        device_id={"tp": device},
        device_id_type=MESH,
    )


def gather_stage(ring, own_ref, whole, sems, prepare, consume):
    width = own_ref.shape[1]
    send, recv, share_send, share_recv = sems

    def columns(device):
        return pl.ds(pl.multiple_of(device * width, width), width)

    hops, shares = {}, {}

    def use(s):
        for j in range(ring.pieces):
            shares[j, s].wait_recv()
        for way in (0, ring.pieces // 2):
            chip = lax.div(ring.device(ring.back(way, s)), 2)
            consume(way * ring.size, chip)

    for s in range(ring.m):
        for j in ring.order():
            rows = ring.piece(j)
            cols = columns(ring.device(ring.back(j, s)))
            if s > 0:
                hops[j, s - 1].wait_recv()
            src = own_ref.at[rows, :] if s == 0 else whole.at[rows, cols]
            if s < ring.m - 1:
                hop = remote(src, whole.at[rows, cols], send.at[j, s], recv.at[j, s], ring.to(j))
                hop.start()
                hops[j, s] = hop
            share = remote(
                src, whole.at[rows, cols], share_send.at[j, s], share_recv.at[j, s], ring.partner
            )
            share.start()
            shares[j, s] = share
        if s == 0:
            whole[:, columns(ring.me)] = own_ref[...]
            prepare()
        else:
            use(s - 1)
    use(ring.m - 1)
    for hop in hops.values():
        hop.wait_send()
    for share in shares.values():
        share.wait_send()


def fill_weights(wq_ref, wk_ref, wv_ref, wg_ref, wcat, total, squares):
    both = 2 * wq_ref.shape[0]
    step = 128

    @pl.loop(0, wcat.shape[0] // step)
    def _(i):
        at = pl.ds(pl.multiple_of(i * step, step), step)
        pair = jnp.concatenate([wq_ref[:, at], wk_ref[:, at]], axis=0)
        wcat[at, :both] = jnp.transpose(pair.astype(F32)).astype(BF16)

    mid = both + wv_ref.shape[1]
    wcat[:, both:mid] = wv_ref[...]
    wcat[:, mid:] = wg_ref[...]
    total[...] = jnp.zeros_like(total)
    squares[...] = jnp.zeros_like(squares)


def consumer(whole, width, gain_ref, wcat, total, squares):
    half = whole.shape[0] // 2
    block = half // 2

    def consume(first, chip):
        cols = pl.ds(pl.multiple_of(chip * 2 * width, 2 * width), 2 * width)
        gain = gain_ref[:, cols]

        @pl.loop(0, 2)
        def _(i):
            at = pl.ds(pl.multiple_of(first + i * block, 16), block)
            x = whole[at, cols].astype(F32)
            square = x * x
            part = square[:, :128]
            for k in range(128, 2 * width, 128):
                part = part + square[:, k : k + 128]
            squares[at, :] += part
            total[at, :] += jnp.dot(
                (x * gain).astype(BF16), wcat[cols, :], preferred_element_type=F32
            )

    return consume


def project_stage(width, total, squares, table_ref, qkv_ref, gate_ref, key_dim):
    rows = total.shape[0]
    both = 2 * key_dim
    value_dim = gate_ref.shape[1]
    block = rows // 4

    @pl.loop(0, 4)
    def _(i):
        at = pl.ds(pl.multiple_of(i * block, block), block)
        mean = jnp.sum(squares[at, :], axis=-1, keepdims=True) / width
        out = total[at, :] * lax.rsqrt(mean + NORM_EPSILON)
        qk = out[:, :both]
        lane = lax.broadcasted_iota(jnp.int32, qk.shape, 1)
        ahead = pltpu.roll(qk, both - key_dim // 2, 1)
        behind = pltpu.roll(qk, key_dim // 2, 1)
        swapped = jnp.where(lax.rem(lane, key_dim) < key_dim // 2, ahead, behind)
        turned = qk * table_ref[at, :both] + swapped * table_ref[at, both:]
        qkv_ref[at, :both] = turned.astype(BF16)
        qkv_ref[at, both:] = out[:, both : both + value_dim].astype(BF16)
        gate = out[:, both + value_dim :]
        gate_ref[at, :] = gate / (1.0 + jnp.exp(-gate))


def scatter_stage(ring, h_ref, w_ref, x_ref, out_ref, h_pair, w_pair, outbox, inbox, sems, prepare):
    width = x_ref.shape[1]
    depth = h_ref.shape[1]
    send, recv, pair_send, pair_recv = sems
    w_copy = remote(
        w_ref, w_pair.at[pl.ds(depth, depth), :], pair_send.at[0], pair_recv.at[0], ring.partner
    )
    w_copy.start()
    h_copy = remote(
        h_ref, h_pair.at[:, pl.ds(depth, depth)], pair_send.at[1], pair_recv.at[1], ring.partner
    )
    h_copy.start()
    prepare()
    w_pair[:depth, :] = w_ref[...]
    h_pair[:, :depth] = h_ref[...]
    w_copy.wait()
    h_copy.wait()
    hops = {}
    for s in range(ring.m):
        for j in ring.order():
            rows = ring.piece(j)
            target = ring.device(ring.back(j, s + 1))
            cols = pl.ds(pl.multiple_of(target * width, width), width)
            part = jnp.dot(h_pair[rows, :], w_pair[:, cols], preferred_element_type=F32)
            if s > 0:
                hops[j, s - 1].wait_recv()
                part = part + inbox[j, s - 1].astype(F32)
            if s < ring.m - 1:
                outbox[j, s] = part.astype(BF16)
                hop = remote(
                    outbox.at[j, s], inbox.at[j, s], send.at[j, s], recv.at[j, s], ring.to(j)
                )
                hop.start()
                hops[j, s] = hop
            else:
                mix = part.astype(BF16).astype(F32)
                out_ref[rows, :] = (x_ref[rows, :].astype(F32) + mix).astype(BF16)
    for hop in hops.values():
        hop.wait_send()


def nothing():
    pass


def first_kernel(n, pieces, key_dim, *refs):
    x_ref, gain_ref, wq, wk, wv, wg, table, qkv, gate, whole, wcat, total, squares, *sems = refs
    ring = Ring(n, x_ref.shape[0], pieces)
    ring.enter()
    fill = functools.partial(fill_weights, wq, wk, wv, wg, wcat, total, squares)
    consume = consumer(whole, x_ref.shape[1], gain_ref, wcat, total, squares)
    gather_stage(ring, x_ref, whole, sems, fill, consume)
    project_stage(whole.shape[1], total, squares, table, qkv, gate, key_dim)


def middle_kernel(n, pieces, key_dim, *refs):
    h_ref, w_ref, x_ref, gain_ref, wq, wk, wv, wg, table = refs[:9]
    x1, qkv, gate, whole, wcat, total, squares, h_pair, w_pair, outbox, inbox = refs[9:20]
    sems = refs[20:]
    ring = Ring(n, x_ref.shape[0], pieces)
    ring.enter()
    fill = functools.partial(fill_weights, wq, wk, wv, wg, wcat, total, squares)
    consume = consumer(whole, x_ref.shape[1], gain_ref, wcat, total, squares)
    scatter_stage(
        ring, h_ref, w_ref, x_ref, x1, h_pair, w_pair, outbox, inbox, sems[4:], fill
    )
    gather_stage(ring, x1, whole, sems[:4], nothing, consume)
    project_stage(whole.shape[1], total, squares, table, qkv, gate, key_dim)


def last_kernel(n, pieces, *refs):
    h_ref, w_ref, x_ref, out_ref, h_pair, w_pair, outbox, inbox, *sems = refs
    ring = Ring(n, x_ref.shape[0], pieces)
    ring.enter()
    scatter_stage(
        ring, h_ref, w_ref, x_ref, out_ref, h_pair, w_pair, outbox, inbox, sems, nothing
    )


def gather_scratch(n, pieces, rows, width, wide):
    scratch = [
        pltpu.VMEM((rows, n * width), BF16),
        pltpu.VMEM((n * width, wide), BF16),
        pltpu.VMEM((rows, wide), F32),
        pltpu.VMEM((rows, 128), F32),
    ]
    m = n // 2
    sems = [pltpu.SemaphoreType.DMA((pieces, m - 1))] * 2 + [pltpu.SemaphoreType.DMA((pieces, m))] * 2
    return scratch, sems


def scatter_scratch(n, pieces, rows, width, depth):
    m = n // 2
    boxes = pltpu.VMEM((pieces, m - 1, rows // pieces, width), BF16)
    scratch = [
        pltpu.VMEM((rows, 2 * depth), BF16),
        pltpu.VMEM((2 * depth, n * width), BF16),
        boxes,
        boxes,
    ]
    sems = [pltpu.SemaphoreType.DMA((pieces, m - 1))] * 2 + [pltpu.SemaphoreType.DMA((2,))] * 2
    return scratch, sems


def call(kernel, outs, scratch, collective_id, *args):
    vmem = pl.BlockSpec(memory_space=pltpu.VMEM)
    return pl.pallas_call(
        kernel,
        out_shape=outs,
        in_specs=[vmem] * len(args),
        out_specs=[vmem] * len(outs),
        scratch_shapes=scratch,
        compiler_params=pltpu.CompilerParams(
            collective_id=collective_id, has_side_effects=True, vmem_limit_bytes=56 * 2**20
        ),
    )(*args)


def plain_project(x, gain, weights, table, key_dim):
    whole = lax.all_gather(x, "tp", axis=1, tiled=True).astype(F32)
    inv = lax.rsqrt(jnp.mean(whole * whole, axis=-1, keepdims=True) + NORM_EPSILON)
    normed = (whole * inv * gain).astype(BF16)
    qk = jnp.dot(normed, jnp.concatenate(weights[:2], axis=1), preferred_element_type=F32)
    halves = qk.reshape(qk.shape[0], 2, 2, key_dim // 2)
    swapped = halves[:, :, ::-1].reshape(qk.shape)
    turned = qk * table[:, : 2 * key_dim] + swapped * table[:, 2 * key_dim :]
    values = jnp.dot(normed, weights[2], preferred_element_type=F32)
    gate = jnp.dot(normed, weights[3], preferred_element_type=F32)
    qkv = jnp.concatenate([turned.astype(BF16), values.astype(BF16)], axis=1)
    return qkv, jax.nn.silu(gate)


def plain_finish(h, w_out, x):
    part = jnp.dot(h, w_out, preferred_element_type=F32).astype(BF16)
    mix = lax.psum_scatter(part, "tp", scatter_dimension=1, tiled=True)
    return (x.astype(F32) + mix.astype(F32)).astype(BF16)


def shards(
    tokens,
    lengths,
    gain_first,
    query_first,
    key_first,
    value_first,
    gate_first,
    out_first,
    state_first,
    gain_second,
    query_second,
    key_second,
    value_second,
    gate_second,
    out_second,
    state_second,
):
    n = lax.axis_size("tp")
    batch_size, head_count, key_dim, value_dim = state_first.shape
    slots, width = tokens.shape
    block_len = slots // batch_size
    rows = LIVE_TOTAL

    lengths_i = lengths.astype(jnp.int32)
    starts = jnp.cumsum(lengths_i) - lengths_i
    slot = jnp.arange(block_len, dtype=jnp.int32)
    live = slot[None, :] < lengths_i[:, None]
    target = jnp.where(live, starts[:, None] + slot[None, :], -1).reshape(slots)
    pack = (jnp.arange(rows, dtype=jnp.int32)[:, None] == target[None, :]).astype(BF16)

    def packed(padded):
        return jnp.dot(pack, padded, preferred_element_type=F32)

    def spread(rows_in):
        return lax.dot_general(
            pack, rows_in, (((0,), (0,)), ((), ())), preferred_element_type=F32
        ).astype(rows_in.dtype)

    slot_hot = jnp.tile(jnp.eye(block_len, dtype=BF16), (batch_size, 1))
    table = jnp.dot(
        packed(slot_hot), rope_tables(block_len, key_dim), precision=lax.Precision.HIGHEST
    )
    x = packed(tokens).astype(BF16)

    weights_first = (query_first, key_first, value_first, gate_first)
    weights_second = (query_second, key_second, value_second, gate_second)
    wide = sum(w.shape[1] for w in weights_first)
    pieces = next((p for p in (10, 6, 4, 2) if rows % (16 * p) == 0), 0)
    ringed = (
        n >= 4
        and n % 2 == 0
        and pieces > 0
        and rows % 64 == 0
        and head_count == 1
        and width % 128 == 0
        and value_dim % 128 == 0
        and 2 * key_dim % 128 == 0
    )
    size = 128
    grouped = (
        head_count == 1
        and size % (2 * block_len) == 0
        and slots % size == 0
        and 2 * key_dim == 128
        and value_dim % 128 == 0
        and rows % 16 == 0
    )
    if grouped:
        log_gamma = decay_logs(1)[0]
        slot_f, count = slot.astype(F32), lengths_i.astype(F32)
        inward = jnp.broadcast_to(jnp.exp(log_gamma * (slot_f + 1.0))[None, :], live.shape)
        gap = jnp.maximum(count[:, None] - 1.0 - slot_f[None, :], 0.0)
        onward = jnp.exp(log_gamma * gap)
        side = jnp.stack([target.astype(F32), inward.reshape(slots), onward.reshape(slots)], axis=1)
        decay = jnp.exp(log_gamma * count)
        r = jnp.arange(size, dtype=jnp.int32)
        step = (r[:, None] - r[None, :]).astype(F32)
        same = (r[:, None] // block_len == r[None, :] // block_len) & (step >= 0.0)
        within = jnp.where(same, jnp.exp(log_gamma * jnp.maximum(step, 0.0)), 0.0)

    def retention(qkv, gate, state):
        if grouped:
            return retain_packed(
                decay, side, target[None, :], within, qkv, gate, state, block_len
            )
        normed, new_state = retain(spread(qkv), lengths, state)
        return (packed(normed) * gate).astype(BF16), new_state

    outs = [
        jax.ShapeDtypeStruct((rows, 2 * key_dim + value_dim), BF16),
        jax.ShapeDtypeStruct((rows, value_dim), F32),
    ]
    own = jax.ShapeDtypeStruct((rows, width), BF16)
    gather_bufs, gather_sems = gather_scratch(n, pieces or 2, rows, width, wide)
    scatter_bufs, scatter_sems = scatter_scratch(n, pieces or 2, rows, width, value_dim)

    def turned(weights):
        return (weights[0].T, weights[1].T) + weights[2:]

    if ringed:
        qkv, gate = call(
            functools.partial(first_kernel, n, pieces, key_dim),
            outs,
            gather_bufs + gather_sems,
            0,
            x,
            gain_first[None],
            *turned(weights_first),
            table,
        )
    else:
        qkv, gate = plain_project(x, gain_first, weights_first, table, key_dim)
    h, state_first_new = retention(qkv, gate, state_first)
    if ringed:
        x1, qkv, gate = call(
            functools.partial(middle_kernel, n, pieces, key_dim),
            [own] + outs,
            gather_bufs + scatter_bufs + gather_sems + scatter_sems,
            1,
            h,
            out_first,
            x,
            gain_second[None],
            *turned(weights_second),
            table,
        )
    else:
        x1 = plain_finish(h, out_first, x)
        qkv, gate = plain_project(x1, gain_second, weights_second, table, key_dim)
    h, state_second_new = retention(qkv, gate, state_second)
    if ringed:
        (y,) = call(
            functools.partial(last_kernel, n, pieces),
            [own],
            scatter_bufs + scatter_sems,
            2,
            h,
            out_second,
            x1,
        )
    else:
        y = plain_finish(h, out_second, x1)
    mixed_out = jnp.where(live.reshape(slots, 1), spread(y), tokens)
    return (mixed_out, state_first_new, state_second_new)


def solution(mesh):
    heads = P(None, "tp")
    state = P("grp", "tp", None, None)
    block = (P(), heads, heads, heads, heads, P("tp", None), state)
    in_specs = (P("grp", "tp"), P("grp")) + block + block
    out_specs = (P("grp", "tp"), state, state)
    return jax.shard_map(shards, mesh=mesh, in_specs=in_specs, out_specs=out_specs, check_vma=False)
```

profile of v0, /device:TPU:0, one launch (start us, length us, event | category | flops | bytes accessed | tf_op | source)
XLA Modules:
  0.0 165.8 jit_solution(1174681591281710253)
XLA Ops:
  0.8 1.2 convert_add_fusion
  2.0 0.1 multiply_exponential_fusion
  2.0 0.7 iota_compare_fusion.10
  2.8 0.1 lt.42
  2.9 0.1 multiply_sine_fusion
  3.0 0.1 maximum_multiply_fusion
  3.1 0.1 concatenate.12
  3.2 0.1 copy.34
  3.3 0.1 exp.29
  3.4 0.1 stack_reshape.4
  3.5 0.8 copy.33
  4.2 0.1 reduce-window.9
  4.3 0.1 reduce
  4.5 0.7 sub.64
  5.1 0.7 exponential_select_fusion.refs_3_
  5.8 0.7 broadcast_select_fusion
  6.6 0.7 select_n.54.refs_2_
  7.3 0.1 convert_element_type.54
  7.4 0.1 add.77
  7.5 2.7 %fusion.8.refs_0_.refs_2_ = bf16[960,128]{1,0:T(8,128)(2,1)} fusion(bf16[1536,128]{1,0:T(8,128)(2,1)} %param.16, s32[1536]{0:T(1024)S(1)} %broadcast_select_fusion.1), kind=kOutput, calls=%fused_computation.9 | convolution fusion | flops 379084800 | bytes 645120 | tf_op jit(solution)/shard_map/dot_general | solution.py:528
  10.2 0.1 tile.4
  10.3 1.1 fusion.1
  11.4 1.2 copy.36.refs_1_
  12.6 1.9 %fusion.13.refs_6_.refs_8_ = f32[960,256]{1,0:T(8,128)} fusion(f32[960,16]{0,1:T(8,128)S(1)} %fusion.1, f32[16,256]{1,0:T(8,128)S(1)} %concatenate.12), kind=kOutput, calls=%fused_computation.38 | convolution fusion | flops 47185920 | bytes 1060864 | tf_op jit(solution)/shard_map/dot_general | solution.py:536
  14.5 35.9 %shard_map.175 = (bf16[960,256]{1,0:T(8,128)(2,1)}, f32[960,128]{1,0:T(8,128)}) custom-call(bf16[960,128]{1,0:T(8,128)(2,1)} %fusion.8.refs_0_.refs_2_, f32[1,2048]{1,0:T(1,128)} %bitcast.28, bf16[64,2048]{1,0:T(8,128)(2,1)} %bitcast.26, bf16[64,2048]{1,0:T(8,128)(2,1)} %bitcast.27, bf16[2048,128]{1,0:T(8,128)(2,1)} %refs_4_.1, bf16[2048,128]{1,0:T(8,128)(2,1)} %refs_5_.1, ...), custom_call_target="tpu_custom_call" | custom-call | tf_op jit(solution)/shard_map/pallas_call | solution.py:464
  50.5 10.0 %shard_map.176 = (bf16[960,128]{1,0:T(8,128)(2,1)}, f32[96,64,128]{2,1,0:T(8,128)}) custom-call(f32[96]{0:T(128)} %get-tuple-element.40.refs_0_, f32[1536,3]{1,0:T(8,128)} %copy.36.refs_1_, s32[1,1536]{1,0:T(1,128)} %select_n.54.refs_2_, f32[128,128]{1,0:T(8,128)} %exponential_select_fusion.refs_3_, bf16[960,256]{1,0:T(8,128)(2,1)} %get-tuple-element.12.refs_4_, ...), custom_call_target="tpu_custom_call" | custom-call | tf_op jit(solution)/shard_map/pallas_call | solution.py:170
  60.4 61.0 %shard_map.177 = (bf16[960,128]{1,0:T(8,128)(2,1)}, bf16[960,256]{1,0:T(8,128)(2,1)}, f32[960,128]{1,0:T(8,128)}) custom-call(bf16[960,128]{1,0:T(8,128)(2,1)} %get-tuple-element.14.refs_0_, bf16[128,2048]{1,0:T(8,128)(2,1)} %refs_1_.2, bf16[960,128]{1,0:T(8,128)(2,1)} %fusion.8.refs_0_.refs_2_, f32[1,2048]{1,0:T(1,128)} %bitcast.29, ...), custom_call_target="tpu_custom_call" | custom-call | tf_op jit(solution)/shard_map/pallas_call | solution.py:464
  121.5 0.0 copy-start
  121.5 10.0 %shard_map.178 = (bf16[960,128]{1,0:T(8,128)(2,1)}, f32[96,64,128]{2,1,0:T(8,128)}) custom-call(f32[96]{0:T(128)} %get-tuple-element.40.refs_0_, f32[1536,3]{1,0:T(8,128)} %copy.36.refs_1_, s32[1,1536]{1,0:T(1,128)} %select_n.54.refs_2_, f32[128,128]{1,0:T(8,128)} %exponential_select_fusion.refs_3_, bf16[960,256]{1,0:T(8,128)(2,1)} %get-tuple-element.15.refs_4_, ...), custom_call_target="tpu_custom_call" | custom-call | tf_op jit(solution)/shard_map/pallas_call | solution.py:170
  131.5 30.7 %shard_map.179 = bf16[960,128]{1,0:T(8,128)(2,1)} custom-call(bf16[960,128]{1,0:T(8,128)(2,1)} %get-tuple-element.17.refs_0_, bf16[128,2048]{1,0:T(8,128)(2,1)} %refs_1_.3, bf16[960,128]{1,0:T(8,128)(2,1)} %get-tuple-element.18.refs_2_), custom_call_target="tpu_custom_call" | custom-call | tf_op jit(solution)/shard_map/pallas_call | solution.py:464
  162.2 0.0 copy-done
  162.2 3.6 %fusion.7 = bf16[1536,128]{1,0:T(8,128)(2,1)} fusion(bf16[1536,128]{1,0:T(8,128)(2,1)S(1)} %copy-done, bf16[960,128]{1,0:T(8,128)(2,1)} %shard_map.179, s32[1536]{0:T(1024)S(1)} %broadcast_select_fusion.1, pred[1536]{0:T(1024)(128)(4,1)S(1)} %lt.42), kind=kOutput, calls=%fused_computation.8 | convolution fusion | flops 379355136 | bytes 1039872 | tf_op jit(solution)/shard_map/dot_general | solution.py:531
  (9 shorter events, 0.1 us)
Async XLA Ops:
  121.5 40.7 %copy-start = (bf16[1536,128]{1,0:T(8,128)(2,1)S(1)}, bf16[1536,128]{1,0:T(8,128)(2,1)}, u32[]{:S(2)}) copy-start(bf16[1536,128]{1,0:T(8,128)(2,1)} %param.16) | copy-start | bytes 1179652
where the time goes:
time: 166 us
  Pallas kernels  148 us (89%)
  matrix products  9.43 us (6%)
  other arithmetic  4.61 us (3%)
  local copies, waits for them, and re-layouts  3.32 us (2%)
    pallas_call x3, Pallas kernels, call(): pl.pallas_call(kernel, out_shape=outs, in_specs=[vmem] * len(args), out_s...  128 us
    pallas_call x2, Pallas kernels, retain_packed(): pl.pallas_call(functools.partial(retention_kernel, key_dim, block_len), g...  19.9 us
    dot_general x2, matrix products, packed(): return jnp.dot(pack, padded, preferred_element_type=F32)  3.88 us
    dot_general x1, matrix products, spread(): lax.dot_general(pack, rows_in, (((0,), (0,)), ((), ())), preferred_elemen...  3.63 us

commit v1 on v0

v1 whole, which is shorter than its diff:
```python
import functools

import jax
import jax.numpy as jnp
from jax import lax
from jax.experimental import pallas as pl
from jax.experimental.pallas import tpu as pltpu
from jax.sharding import PartitionSpec as P
import numpy as np

PAST_LEN = 16384
LIVE_TOTAL = 960

NORM_EPSILON = 1e-06
ROPE_BASE = 10000.0

MESH = pl.DeviceIdType.MESH
F32 = jnp.float32
BF16 = jnp.bfloat16


def decay_logs(head_count):
    head_total = lax.axis_size("tp") * head_count
    head_ids = (lax.axis_index("tp") * head_count + jnp.arange(head_count)).astype(F32)
    return jnp.log(1.0 - 2.0 ** (-1.5 - 6.0 * head_ids / (head_total - 1)))


def rope_tables(block_len, key_dim):
    half_dim = key_dim // 2
    inverse = ROPE_BASE ** (-jnp.arange(half_dim, dtype=F32) / half_dim)
    positions = PAST_LEN + jnp.arange(block_len, dtype=F32)
    angles = positions[:, None] * inverse[None, :]
    cosines, sines = jnp.cos(angles), jnp.sin(angles)
    cosines = jnp.concatenate([cosines, cosines], axis=1)
    sines = jnp.concatenate([-sines, sines], axis=1)
    scale = key_dim ** (-0.5)
    return jnp.concatenate([cosines, cosines * scale, sines, sines * scale], axis=1)


def retain(queries, key_rows, values, lengths, state_in):
    batch_size, head_count, key_dim, value_dim = state_in.shape
    block_len = queries.shape[0] // batch_size
    log_gamma = decay_logs(head_count)
    queries = queries.reshape(batch_size, block_len, head_count, key_dim)
    key_rows = key_rows.reshape(batch_size, block_len, head_count, key_dim)
    values = values.reshape(batch_size, block_len, head_count, value_dim)
    slot_ids = jnp.arange(block_len).astype(F32)
    live_count = lengths.astype(F32)
    active = (slot_ids[None, :] < live_count[:, None]).astype(F32)
    step_gap = slot_ids[:, None] - slot_ids[None, :]
    causal = (step_gap >= 0.0).astype(F32)
    within = jnp.exp(log_gamma[:, None, None] * jnp.maximum(step_gap, 0.0)[None]) * causal[None]
    scores = jnp.einsum("bihd,bjhd->bhij", queries, key_rows, preferred_element_type=F32)
    weights = (scores * within[None]).astype(BF16)
    inner_part = jnp.einsum("bhij,bjhe->bihe", weights, values, preferred_element_type=F32)
    carried = jnp.einsum(
        "bihd,bhde->bihe", queries.astype(F32), state_in, precision=lax.Precision.HIGHEST
    )
    carried = (
        carried * jnp.exp(log_gamma[None, None, :] * (slot_ids[None, :, None] + 1.0))[..., None]
    )
    retained = (inner_part + carried) * active[:, :, None, None]
    lead_gap = live_count[:, None] - 1.0 - slot_ids[None, :]
    key_weight = (
        jnp.exp(log_gamma[None, None, :] * jnp.maximum(lead_gap, 0.0)[:, :, None])
        * active[:, :, None]
    )
    added_state = jnp.einsum(
        "bjhd,bjhe->bhde",
        key_rows.astype(F32) * key_weight[..., None],
        values.astype(F32),
        precision=lax.Precision.HIGHEST,
    )
    new_state = (
        state_in * jnp.exp(log_gamma[None, :] * live_count[:, None])[:, :, None, None] + added_state
    )
    inv_rms = lax.rsqrt(jnp.mean(retained * retained, axis=-1, keepdims=True) + NORM_EPSILON)
    return (retained * inv_rms).reshape(batch_size * block_len, -1), new_state


def rotated(vectors, table, scale_at):
    key_dim = vectors.shape[-1]
    half = key_dim // 2
    swapped = jnp.concatenate([vectors[..., half:], vectors[..., :half]], axis=-1)
    cosines = table[:, None, scale_at * key_dim : (scale_at + 1) * key_dim]
    sines = table[:, None, (2 + scale_at) * key_dim : (3 + scale_at) * key_dim]
    return (vectors * cosines + swapped * sines).astype(BF16)


def plain_block(x, lengths, gain, qk_weights, w_value, w_gate, w_out, state, table):
    batch_size, head_count, key_dim, value_dim = state.shape
    whole = lax.all_gather(x, "tp", axis=1, tiled=True).astype(F32)
    inv = lax.rsqrt(jnp.mean(whole * whole, axis=-1, keepdims=True) + NORM_EPSILON)
    normed = (whole * inv * gain).astype(BF16)
    turned = []
    for scale_at, weight in enumerate(qk_weights):
        product = jnp.einsum("rd,dhk->rhk", normed, weight, preferred_element_type=F32)
        turned.append(rotated(product, table, scale_at))
    values = jnp.dot(normed, w_value, preferred_element_type=F32).astype(BF16)
    gate = jnp.dot(normed, w_gate, preferred_element_type=F32)
    retained, new_state = retain(turned[0], turned[1], values, lengths, state)
    heads_out = (retained * jax.nn.silu(gate)).astype(BF16)
    part = jnp.dot(heads_out, w_out, preferred_element_type=F32).astype(BF16)
    mix = lax.psum_scatter(part, "tp", scatter_dimension=1, tiled=True)
    return (x.astype(F32) + mix.astype(F32)).astype(BF16), new_state


FRONT = 32


class Plan:
    def __init__(self, n, rows, pieces, batch, block_len, key_dim, value_dim, width):
        self.n, self.m = n, n // 2
        self.rows, self.pieces, self.size = rows, pieces, rows // pieces
        self.batch, self.block_len = batch, block_len
        self.key_dim, self.value_dim, self.width = key_dim, value_dim, width
        self.slots = batch * block_len
        self.unit = 128
        self.units = self.slots // self.unit
        self.group = self.unit // block_len
        self.long = -(-(rows + FRONT) // 128) * 128
        half, quarter = pieces // 2, pieces // 4
        self.cw = [j for j in range(pieces) if j < quarter or j >= quarter + half]
        self.ccw = [j for j in range(pieces) if quarter <= j < quarter + half]
        self.blocks = [(0, quarter), (quarter, half), (half, quarter + half), (quarter + half, pieces)]
        self.order = [j for pair in zip(self.cw, self.ccw) for j in pair]

    def clockwise(self, j):
        return j in self.cw

    def piece(self, j):
        return pl.ds(j * self.size, self.size)

    def span(self, block):
        return pl.ds(block[0] * self.size, (block[1] - block[0]) * self.size)

    def first_sequence(self, row):
        return max(row // self.block_len, self.batch - self.rows + row)

    def last_sequence(self, row):
        return min(row, self.batch - -(-(self.rows - row) // self.block_len))


class Ring:
    def __init__(self, plan):
        self.plan, self.m = plan, plan.m
        me = lax.axis_index("tp")
        self.core = lax.rem(me, 2)
        chip = lax.div(me, 2)
        odd = lax.rem(chip, 2)
        half = lax.div(chip, 2)
        self.pos = (1 - odd) * half + odd * (self.m - 1 - half)
        self.me = me
        self.partner = chip * 2 + 1 - self.core
        self.right = self.device(self.pos + 1)
        self.left = self.device(self.pos - 1)

    def device(self, pos):
        m = self.m
        pos = lax.rem(pos + m, m)
        far = lax.div(pos, (m + 1) // 2)
        chip = (1 - far) * 2 * pos + far * (2 * (m - 1 - pos) + 1)
        return chip * 2 + self.core

    def greet(self):
        barrier = pltpu.get_barrier_semaphore()
        for device in (self.left, self.right, self.partner):
            pl.semaphore_signal(barrier, inc=1, device_id={"tp": device}, device_id_type=MESH)

    def met(self):
        pl.semaphore_wait(pltpu.get_barrier_semaphore(), 3)

    def to(self, j):
        return self.right if self.plan.clockwise(j) else self.left

    def origin(self, j, steps):
        back = self.pos - steps if self.plan.clockwise(j) else self.pos + steps
        return self.device(back)


def remote(src, dst, send, recv, device):
    return pltpu.make_async_remote_copy(
        src_ref=src,
        dst_ref=dst,
        send_sem=send,
        recv_sem=recv,
        device_id={"tp": device},
        device_id_type=MESH,
    )


def share_out(step, steps, total, work):
    per = -(-total // steps)
    for k in range(per):
        u = (step - 1) * per + k

        @pl.when(u < total)
        def _():
            work(u)


class Gather:
    def __init__(self, ring, own, whole, sems):
        self.ring, self.plan, self.own, self.whole = ring, ring.plan, own, whole
        self.send, self.recv, self.share_send, self.share_recv = sems

    def columns(self, device):
        return pl.ds(pl.multiple_of(device * self.plan.width, self.plan.width), self.plan.width)

    def place(self, j, s):
        return self.whole.at[self.plan.piece(j), self.columns(self.ring.origin(j, s))]

    def source(self, j, s):
        if isinstance(s, int) and s == 0:
            return self.own.at[self.plan.piece(j), :]
        return self.place(j, s)

    def hop(self, j, s):
        return remote(
            self.source(j, s), self.place(j, s), self.send.at[j, s], self.recv.at[j, s], self.ring.to(j)
        )

    def share(self, j, s):
        return remote(
            self.source(j, s),
            self.place(j, s),
            self.share_send.at[j, s],
            self.share_recv.at[j, s],
            self.ring.partner,
        )

    def begin(self, j):
        self.hop(j, 0).start()
        self.share(j, 0).start()
        self.whole[self.plan.piece(j), self.columns(self.ring.me)] = self.own[self.plan.piece(j), :]

    def forward(self, j, s, last):
        self.hop(j, s - 1).wait_recv()
        if not last:
            self.hop(j, s).start()
        self.share(j, s).start()

    def drain(self):
        for j in range(self.plan.pieces):
            self.hop(j, 0).wait_send()
            self.share(j, 0).wait_send()

        @pl.loop(1, self.plan.m - 1)
        def _(s):
            for j in range(self.plan.pieces):
                self.hop(j, s).wait_send()
                self.share(j, s).wait_send()

        for j in range(self.plan.pieces):
            self.share(j, self.plan.m - 1).wait_send()


class Projection:
    def __init__(self, gather, gain, wcat, total, squares):
        self.gather, self.plan, self.ring = gather, gather.plan, gather.ring
        self.gain, self.wcat, self.total, self.squares = gain, wcat, total, squares

    def product(self, block, s):
        plan = self.plan
        for j in range(*block):
            self.gather.share(j, s).wait_recv()
        chip = lax.div(self.ring.origin(block[0], s), 2)
        cols = pl.ds(pl.multiple_of(chip * 2 * plan.width, 2 * plan.width), 2 * plan.width)
        x = self.gather.whole[plan.span(block), cols].astype(F32)
        square = x * x
        part = square[:, :128]
        for k in range(128, 2 * plan.width, 128):
            part = part + square[:, k : k + 128]
        scaled = (x * self.gain[:, cols]).astype(BF16)
        return jnp.dot(scaled, self.wcat[cols, :], preferred_element_type=F32), part

    def first(self, block):
        at = self.plan.span(block)
        self.total[at, :], self.squares[at, :] = self.product(block, 0)

    def add(self, block, s):
        at = self.plan.span(block)
        product, part = self.product(block, s)
        self.total[at, :] += product
        self.squares[at, :] += part

    def finish(self, block, table, queries, kv, gate):
        plan = self.plan
        at = plan.span(block)
        product, part = self.product(block, plan.m - 1)
        square = self.squares[at, :] + part
        mean = jnp.sum(square, axis=-1, keepdims=True) / (plan.n * plan.width)
        out = (self.total[at, :] + product) * lax.rsqrt(mean + NORM_EPSILON)
        key_dim, both = plan.key_dim, 2 * plan.key_dim
        qk = out[:, :both]
        lane = lax.broadcasted_iota(jnp.int32, qk.shape, 1)
        ahead = pltpu.roll(qk, both - key_dim // 2, 1)
        behind = pltpu.roll(qk, key_dim // 2, 1)
        swapped = jnp.where(lax.rem(lane, key_dim) < key_dim // 2, ahead, behind)
        turned = qk * table[at, :both] + swapped * table[at, both:]
        crossed = pltpu.roll(turned, key_dim, 1)
        front = lane < key_dim
        queries[at, :] = jnp.where(front, turned, crossed).astype(BF16)
        low = pl.ds(FRONT + block[0] * plan.size, (block[1] - block[0]) * plan.size)
        kv[low, :both] = jnp.where(front, crossed, turned).astype(BF16)
        kv[low, both:] = out[:, both : both + plan.value_dim].astype(BF16)
        open_gate = out[:, both + plan.value_dim :]
        gate[at, :] = open_gate / (1.0 + jnp.exp(-open_gate))


def fill_unit(wq, wk, wcat, u):
    at = pl.ds(pl.multiple_of(u * 128, 128), 128)
    pair = jnp.concatenate([wq[:, at], wk[:, at]], axis=0)
    wcat[at, : 2 * wq.shape[0]] = jnp.transpose(pair.astype(F32)).astype(BF16)


def pack_rows(plan, lens_ref, tokens, x, trow, bounds, send):
    lens = jnp.broadcast_to(lens_ref[...].astype(F32), (8, plan.batch)).astype(BF16)
    wide = (plan.batch, plan.slots)
    sequence = lax.broadcasted_iota(jnp.int32, wide, 0)
    owner = lax.div(lax.broadcasted_iota(jnp.int32, wide, 1), plan.block_len)
    before = jnp.where(sequence < owner, 1.0, 0.0).astype(BF16)
    same = jnp.where(sequence == owner, 1.0, 0.0).astype(BF16)
    start = jnp.dot(lens, before, preferred_element_type=F32)
    count = jnp.dot(lens, same, preferred_element_type=F32)
    slot = lax.rem(lax.broadcasted_iota(jnp.int32, start.shape, 1), plan.block_len).astype(F32)
    trow[...] = jnp.where(slot < count, start + slot, -1.0)
    square = (plan.batch, plan.batch)
    earlier = lax.broadcasted_iota(jnp.int32, square, 0) < lax.broadcasted_iota(jnp.int32, square, 1)
    begin = jnp.dot(lens, jnp.where(earlier, 1.0, 0.0).astype(BF16), preferred_element_type=F32)
    bounds[0:8, :] = begin
    bounds[8:16, :] = begin + lens.astype(F32)
    base = lax.broadcasted_iota(jnp.int32, (plan.size, plan.slots), 0).astype(F32)
    for j in plan.order:
        hot = jnp.where(base + float(j * plan.size) == trow[0:1, :], 1.0, 0.0).astype(BF16)
        x[plan.piece(j), :] = jnp.dot(hot, tokens[...], preferred_element_type=F32).astype(BF16)
        send(j)


def row_unit(plan, bounds, rope, tcol, bcol, table, u):
    at = pl.ds(pl.multiple_of(u * plan.size, plan.size), plan.size)
    shape = (plan.size, plan.batch)
    row = (lax.broadcasted_iota(jnp.int32, shape, 0) + u * plan.size).astype(F32)
    begin, end = bounds[0:1, :], bounds[8:9, :]
    inside = (row >= begin) & (row < end)
    slot = jnp.sum(jnp.where(inside, row - begin, 0.0), axis=-1, keepdims=True)
    owner = jnp.sum(jnp.where(row >= end, 1.0, 0.0), axis=-1, keepdims=True)
    full = (plan.size, 128)
    slot = jnp.broadcast_to(slot, full)
    tcol[at, :] = slot
    bcol[at, :] = jnp.broadcast_to(owner, full).astype(BF16)
    lane = lax.broadcasted_iota(jnp.int32, full, 1)
    pick = (lax.rem(lane, plan.block_len).astype(F32) == slot) & (lane < 3 * plan.block_len)
    pick = jnp.where(pick, 1.0, 0.0).astype(BF16)
    table[at, :] = jnp.dot(pick, rope[...], preferred_element_type=F32)


def slot_unit(plan, rate, lens_ref, tgt, onward, hot, u):
    at = pl.ds(pl.multiple_of(u * plan.unit, plan.unit), plan.unit)
    lens = jnp.broadcast_to(lens_ref[...].astype(F32), (plan.unit, plan.batch)).astype(BF16)
    shape = (plan.unit, plan.batch)
    owner = lax.div(lax.broadcasted_iota(jnp.int32, shape, 0), plan.block_len) + u * plan.group
    sequence = lax.broadcasted_iota(jnp.int32, shape, 1)
    before = jnp.where(sequence < owner, 1.0, 0.0).astype(BF16)
    same = jnp.where(sequence == owner, 1.0, 0.0).astype(BF16)
    dims = (((1,), (1,)), ((), ()))
    start = lax.dot_general(before, lens, dims, preferred_element_type=F32)
    count = lax.dot_general(same, lens, dims, preferred_element_type=F32)
    full = (plan.unit, plan.unit)
    slot = lax.rem(lax.broadcasted_iota(jnp.int32, full, 0), plan.block_len).astype(F32)
    target = jnp.where(slot < count, start + slot, -1.0)
    tgt[at, :] = target
    onward[at, :] = jnp.exp(rate * jnp.maximum(count - 1.0 - slot, 0.0))
    moved = jnp.where(target >= 0.0, target + float(FRONT), -1.0)
    lane = lax.broadcasted_iota(jnp.int32, full, 1).astype(F32)
    for c in range(plan.long // 128):
        hot[at, c * 128 : (c + 1) * 128] = jnp.where(moved == lane + float(c * 128), 1.0, 0.0).astype(BF16)


def split_unit(plan, state, halves, u):
    at = pl.ds(pl.multiple_of(u * plan.group, plan.group), plan.group)
    rows = plan.group * plan.key_dim
    whole = state[at].reshape(rows, plan.value_dim)
    high = whole.astype(BF16)
    to = pl.ds(pl.multiple_of(u * rows, rows), rows)
    halves[to, : plan.value_dim] = high
    halves[to, plan.value_dim :] = (whole - high.astype(F32)).astype(BF16)


def state_unit(plan, lens_smem, powers, me, hot, kv, onward, state, u):
    at = pl.ds(pl.multiple_of(u * plan.unit, plan.unit), plan.unit)
    both = 2 * plan.key_dim
    padded = jnp.dot(hot[at, :], kv[...], preferred_element_type=F32)
    values = padded[:, both:].astype(BF16)
    scaled = padded[:, :both] * onward[at, :]
    high = scaled.astype(BF16).astype(F32)
    wide = (plan.unit, plan.group * plan.key_dim)
    own = lax.div(lax.broadcasted_iota(jnp.int32, wide, 0), plan.block_len) == lax.div(
        lax.broadcasted_iota(jnp.int32, wide, 1), plan.key_dim
    )
    added = None
    for piece in (high, scaled - high):
        spread = jnp.where(own, jnp.concatenate([piece] * (plan.group // 2), axis=1), 0.0)
        term = lax.dot_general(
            spread.astype(BF16), values, (((0,), (0,)), ((), ())), preferred_element_type=F32
        )
        added = term if added is None else added + term
    for b in range(plan.group):
        which = u * plan.group + b
        decay = powers[me, lens_smem[which]]
        state[which] = state[which] * decay + added[b * plan.key_dim : (b + 1) * plan.key_dim, :]


def retention_block(plan, rate, block, queries, kv, gate, tcol, bcol, fade, halves):
    both = 2 * plan.key_dim
    inner = []
    shape = (plan.size, 128)
    gap = lax.broadcasted_iota(jnp.int32, shape, 0) - lax.broadcasted_iota(jnp.int32, shape, 1)
    gap = (gap + FRONT).astype(F32)
    for j in range(*block):
        window = pl.ds(j * plan.size, 128)
        scores = lax.dot_general(
            queries[plan.piece(j), :],
            kv[window, :both],
            (((1,), (1,)), ((), ())),
            preferred_element_type=F32,
        )
        weights = jnp.where(gap <= tcol[plan.piece(j), :], scores * fade[...], 0.0).astype(BF16)
        inner.append(jnp.dot(weights, kv[window, both:], preferred_element_type=F32))
    at = plan.span(block)
    low = plan.first_sequence(block[0] * plan.size) // 2
    high = plan.last_sequence(block[1] * plan.size - 1) // 2 + 1
    q, owner = queries[at, :], bcol[at, :]
    lane = lax.broadcasted_iota(jnp.int32, (q.shape[0], both), 1)
    pick = owner - jnp.where(lane < plan.key_dim, 0.0, 1.0).astype(BF16)
    zero = jnp.zeros_like(q)
    spread = [jnp.where(pick == jnp.asarray(2.0 * c, BF16), q, zero) for c in range(low, high)]
    carried = jnp.dot(
        jnp.concatenate(spread, axis=1),
        halves[low * both : high * both, :],
        preferred_element_type=F32,
    )
    carried = carried[:, : plan.value_dim] + carried[:, plan.value_dim :]
    retained = jnp.concatenate(inner, axis=0) + carried * jnp.exp(rate * (tcol[at, :] + 1.0))
    inv = lax.rsqrt(jnp.mean(retained * retained, axis=-1, keepdims=True) + NORM_EPSILON)
    return (retained * inv * gate[at, :]).astype(BF16)


class Scatter:
    def __init__(self, ring, h_pair, w_pair, outbox, inbox, parts, sems):
        self.ring, self.plan = ring, ring.plan
        self.h_pair, self.w_pair, self.outbox, self.inbox, self.parts = h_pair, w_pair, outbox, inbox, parts
        self.send, self.recv, self.pair_send, self.pair_recv = sems

    def offer(self, k):
        rows, depth = self.plan.span(self.plan.blocks[k]), self.plan.value_dim
        return remote(
            self.h_pair.at[rows, pl.ds(0, depth)],
            self.h_pair.at[rows, pl.ds(depth, depth)],
            self.pair_send.at[k],
            self.pair_recv.at[k],
            self.ring.partner,
        )

    def hop(self, j, s):
        return remote(
            self.outbox.at[j, s],
            self.inbox.at[j, s],
            self.send.at[j, s],
            self.recv.at[j, s],
            self.ring.to(j),
        )

    def product(self, k, s):
        block, width = self.plan.blocks[k], self.plan.width
        target = self.ring.origin(block[0], s + 1)
        cols = pl.ds(pl.multiple_of(target * width, width), width)
        return jnp.dot(
            self.h_pair[self.plan.span(block), :], self.w_pair[:, cols], preferred_element_type=F32
        )

    def begin(self, k):
        self.offer(k).wait_recv()
        part = self.product(k, 0).astype(BF16)
        first, last = self.plan.blocks[k]
        for j in range(first, last):
            self.outbox[j, 0] = part[(j - first) * self.plan.size : (j - first + 1) * self.plan.size, :]
            self.hop(j, 0).start()

    def prepare(self, k, s):
        self.parts[lax.rem(s, 2), self.plan.span(self.plan.blocks[k]), :] = self.product(k, s)

    def take(self, j, s):
        self.hop(j, s - 1).wait_recv()
        return self.parts[lax.rem(s, 2), self.plan.piece(j), :] + self.inbox[j, s - 1].astype(F32)

    def forward(self, j, s):
        self.outbox[j, s] = self.take(j, s).astype(BF16)
        self.hop(j, s).start()

    def steps(self, work):
        for k in range(4):
            self.prepare(k, 1)

        @pl.loop(1, self.plan.m - 1)
        def _(s):
            for i, j in enumerate(self.plan.order):
                self.forward(j, s)
                if i % 2 == 1 and i < 8:
                    self.prepare(i // 2, s + 1)
            for i in range(len(self.plan.order) // 2, 4):
                self.prepare(i, s + 1)
            work(s)

    def last(self, j):
        return self.take(j, self.plan.m - 1).astype(BF16).astype(F32)

    def drain(self):
        for k in range(4):
            self.offer(k).wait_send()

        @pl.loop(0, self.plan.m - 1)
        def _(s):
            for j in range(self.plan.pieces):
                self.hop(j, s).wait_send()


def whole_kernel(plan, *refs):
    (lens_smem, powers, rates, lens_ref, tokens, rope, *rest) = refs
    gains, raw, outs_w, states_in, (mixed, *states_out), scratch = (
        (rest[0], rest[7]),
        (rest[1:5], rest[8:12]),
        (rest[5], rest[12]),
        (rest[6], rest[13]),
        rest[14:17],
        rest[17:],
    )
    (x, x1, y, whole, wcats, turned, w_pairs, total, squares, table, gate, tcol, bcol, queries) = scratch[:14]
    (kv, halves, states, hot, onward, tgt, parts, outbox, inbox, h_pair, trow, bounds, fade) = scratch[14:27]
    load, store, pair_w = scratch[27:30]
    sems = scratch[30:]
    ring = Ring(plan)
    ring.greet()
    depth, both = plan.value_dim, 2 * plan.key_dim
    rate = rates[0, ring.me]

    loads = {}
    for i in range(2):
        wq, wk, wv, wg = raw[i]
        targets = (
            (wq, turned.at[i, 0]),
            (wk, turned.at[i, 1]),
            (wv, wcats.at[i, :, pl.ds(both, depth)]),
            (wg, wcats.at[i, :, pl.ds(both + depth, depth)]),
            (outs_w[i], w_pairs.at[i, pl.ds(0, depth), :]),
            (states_in[i], states.at[i]),
        )
        for k, (source, target) in enumerate(targets):
            loads[i, k] = pltpu.make_async_copy(source, target, load.at[i, k])

    def swap(i):
        return remote(
            w_pairs.at[i, pl.ds(0, depth), :],
            w_pairs.at[i, pl.ds(depth, depth), :],
            pair_w.at[0, i],
            pair_w.at[1, i],
            ring.partner,
        )

    gathers = [Gather(ring, (x, x1)[i], whole, sems[8 * i : 8 * i + 4]) for i in range(2)]
    scatters = [
        Scatter(ring, h_pair, w_pairs.at[i], outbox, inbox, parts, sems[8 * i + 4 : 8 * i + 8])
        for i in range(2)
    ]
    projections = [Projection(gathers[i], gains[i], wcats.at[i], total, squares) for i in range(2)]

    for k in range(6):
        loads[0, k].start()
    met = []

    def send(j):
        if not met:
            ring.met()
            met.append(1)
        gathers[0].begin(j)

    pack_rows(plan, lens_ref, tokens, x, trow, bounds, send)
    for k in range(6):
        loads[1, k].start()
    loads[0, 0].wait()
    loads[0, 1].wait()

    @pl.loop(0, wcats.shape[1] // 128)
    def _(u):
        fill_unit(turned.at[0, 0], turned.at[0, 1], wcats.at[0], u)

    loads[0, 2].wait()
    loads[0, 3].wait()
    shape = (plan.size, 128)
    gap = lax.broadcasted_iota(jnp.int32, shape, 0) - lax.broadcasted_iota(jnp.int32, shape, 1)
    gap = (gap + FRONT).astype(F32)
    near = (gap >= 0.0) & (gap < float(plan.block_len))
    fade[...] = jnp.where(near, 0.5 * jnp.exp(rate * jnp.maximum(gap, 0.0)), 0.0)
    kv[:FRONT, :] = jnp.zeros((FRONT, kv.shape[1]), BF16)
    kv[FRONT + plan.rows :, :] = jnp.zeros((plan.long - FRONT - plan.rows, kv.shape[1]), BF16)
    y[:FRONT, :] = jnp.zeros((FRONT, plan.width), BF16)
    y[FRONT + plan.rows :, :] = jnp.zeros((plan.long - FRONT - plan.rows, plan.width), BF16)
    loads[0, 5].wait()
    loads[0, 4].wait()
    swap(0).start()

    def run(i, gather_work, before_last, scatter_work, finish):
        gather, projection, scatter = gathers[i], projections[i], scatters[i]
        m, blocks = plan.m, plan.blocks

        def gather_step(s, last):
            for k, j in enumerate(plan.order):
                gather.forward(j, s, last)
                if k % 2 == 1 and k < 8:
                    if isinstance(s, int) and s == 1:
                        projection.first(blocks[k // 2])
                    else:
                        projection.add(blocks[k // 2], s - 1)
            for k in range(len(plan.order) // 2, 4):
                if isinstance(s, int) and s == 1:
                    projection.first(blocks[k])
                else:
                    projection.add(blocks[k], s - 1)

        gather_step(1, False)
        gather_work(1)

        @pl.loop(2, m - 1)
        def _(s):
            gather_step(s, False)
            gather_work(s)

        gather_step(m - 1, True)
        before_last()
        gather.drain()

        def retain_block(k):
            block = blocks[k]
            projection.finish(block, table, queries, kv, gate)
            h_pair[plan.span(block), :depth] = retention_block(
                plan, rate, block, queries, kv, gate, tcol, bcol, fade, halves
            )
            scatter.offer(k).start()

        retain_block(0)
        retain_block(1)
        swap(i).wait_recv()
        scatter.begin(0)
        retain_block(2)
        scatter.begin(1)
        retain_block(3)
        scatter.begin(2)
        scatter.begin(3)
        scatter.steps(scatter_work)
        for j in plan.order:
            finish(j, scatter.last(j))
        scatter.drain()
        swap(i).wait_send()

    def first_gather(s):
        share_out(s, plan.m - 2, plan.pieces, lambda u: row_unit(plan, bounds, rope, tcol, bcol, table, u))
        share_out(s, plan.m - 2, plan.units, lambda u: split_unit(plan, states.at[0], halves, u))
        share_out(
            s, plan.m - 2, plan.units, lambda u: slot_unit(plan, rate, lens_ref, tgt, onward, hot, u)
        )

    def update(i, s):
        share_out(
            s,
            plan.m - 2,
            plan.units,
            lambda u: state_unit(plan, lens_smem, powers, ring.me, hot, kv, onward, states.at[i], u),
        )

    def first_scatter(s):
        update(0, s)

    def after_first(j, mix):
        at = plan.piece(j)
        x1[at, :] = (x[at, :].astype(F32) + mix).astype(BF16)
        gathers[1].begin(j)

    run(0, first_gather, lambda: None, first_scatter, after_first)
    save = pltpu.make_async_copy(states.at[0], states_out[0], store.at[0])
    save.start()
    for k in range(6):
        loads[1, k].wait()
    swap(1).start()

    @pl.loop(0, wcats.shape[1] // 128)
    def _(u):
        fill_unit(turned.at[1, 0], turned.at[1, 1], wcats.at[1], u)

    def second_gather(s):
        share_out(s, plan.m - 2, plan.units, lambda u: split_unit(plan, states.at[1], halves, u))

    def after_second(j, mix):
        at = plan.piece(j)
        y[pl.ds(FRONT + j * plan.size, plan.size), :] = (x1[at, :].astype(F32) + mix).astype(BF16)

    run(1, second_gather, lambda: None, lambda s: update(1, s), after_second)
    save_second = pltpu.make_async_copy(states.at[1], states_out[1], store.at[1])
    save_second.start()
    many = next(k for k in (3, 2, 1) if plan.units % k == 0)

    @pl.loop(0, plan.units // many)
    def _(u):
        at = pl.ds(pl.multiple_of(u * many * plan.unit, plan.unit), many * plan.unit)
        spread = jnp.dot(hot[at, :], y[...], preferred_element_type=F32)
        live = jnp.concatenate([tgt[at, :]] * (plan.width // 128), axis=1) >= 0.0
        mixed[at, :] = jnp.where(live, spread, tokens[at, :].astype(F32)).astype(BF16)

    save.wait()
    save_second.wait()


def fused(plan, heads, lengths, tokens, first, second):
    total_heads = heads
    logs = np.log(1.0 - 2.0 ** (-1.5 - 6.0 * np.arange(total_heads) / (total_heads - 1)))
    powers = np.exp(logs[:, None] * np.arange(plan.block_len + 1)[None, :]).astype(np.float32)
    half = plan.key_dim // 2
    inverse = np.float32(ROPE_BASE) ** (-np.arange(half, dtype=np.float32) / np.float32(half))
    positions = PAST_LEN + np.arange(plan.block_len, dtype=np.float32)
    angles = (positions[:, None] * inverse.astype(np.float32)[None, :]).astype(np.float64)
    cosines, sines = np.cos(angles), np.sin(angles)
    cosines = np.concatenate([cosines, cosines], axis=1)
    sines = np.concatenate([-sines, sines], axis=1)
    scale = plan.key_dim**-0.5
    rope = np.concatenate([cosines, cosines * scale, sines, sines * scale], axis=1).astype(np.float32)
    stacked, rest = [], rope
    for _ in range(3):
        stacked.append(rest.astype(jnp.bfloat16))
        rest = rest - stacked[-1].astype(np.float32)
    rope = np.zeros((128, rope.shape[1]), jnp.bfloat16)
    rope[: 3 * plan.block_len] = np.concatenate(stacked, axis=0)

    n, m, rows, width = plan.n, plan.m, plan.rows, plan.width
    wide, both = 2 * plan.key_dim + 2 * plan.value_dim, 2 * plan.key_dim
    depth = plan.value_dim
    model = n * width
    state_shape = (plan.batch, plan.key_dim, plan.value_dim)
    vmem = lambda shape, kind: pltpu.VMEM(shape, kind)
    dma = lambda *shape: pltpu.SemaphoreType.DMA(shape)
    scratch = [
        vmem((rows, width), BF16),
        vmem((rows, width), BF16),
        vmem((plan.long, width), BF16),
        vmem((rows, model), BF16),
        vmem((2, model, wide), BF16),
        vmem((2, 2, plan.key_dim, model), BF16),
        vmem((2, 2 * depth, model), BF16),
        vmem((rows, wide), F32),
        vmem((rows, 128), F32),
        vmem((rows, 2 * both), F32),
        vmem((rows, depth), F32),
        vmem((rows, 128), F32),
        vmem((rows, 128), BF16),
        vmem((rows, both), BF16),
        vmem((plan.long, both + depth), BF16),
        vmem((plan.batch * plan.key_dim, 2 * depth), BF16),
        vmem((2,) + state_shape, F32),
        vmem((plan.slots, plan.long), BF16),
        vmem((plan.slots, 128), F32),
        vmem((plan.slots, 128), F32),
        vmem((2, rows, width), F32),
        vmem((plan.pieces, m - 1, plan.size, width), BF16),
        vmem((plan.pieces, m - 1, plan.size, width), BF16),
        vmem((rows, 2 * depth), BF16),
        vmem((8, plan.slots), F32),
        vmem((16, plan.batch), F32),
        vmem((plan.size, 128), F32),
        dma(2, 6),
        dma(2),
        dma(2, 2),
    ]
    for _ in range(2):
        scratch += [dma(plan.pieces, m - 1)] * 2 + [dma(plan.pieces, m)] * 2
        scratch += [dma(plan.pieces, m - 1)] * 2 + [dma(4)] * 2
    spec = lambda space: pl.BlockSpec(memory_space=space)
    inside, outside, scalars = spec(pltpu.VMEM), spec(pltpu.HBM), spec(pltpu.SMEM)

    def group(gain, query, key, value, gate, out, state):
        return (gain[None], query.T, key.T, value, gate, out, state.reshape(state_shape))

    block_specs = [inside] + [outside] * 6
    mixed, one, two = pl.pallas_call(
        functools.partial(whole_kernel, plan),
        out_shape=[
            jax.ShapeDtypeStruct((plan.slots, width), BF16),
            jax.ShapeDtypeStruct(state_shape, F32),
            jax.ShapeDtypeStruct(state_shape, F32),
        ],
        in_specs=[scalars] * 3 + [inside] * 3 + block_specs * 2,
        out_specs=[inside, outside, outside],
        scratch_shapes=scratch,
        compiler_params=pltpu.CompilerParams(
            collective_id=0, has_side_effects=True, vmem_limit_bytes=62 * 2**20
        ),
    )(
        lengths,
        jnp.asarray(powers),
        jnp.asarray(logs.astype(np.float32)[None, :]),
        lengths[None, :],
        tokens,
        jnp.asarray(rope),
        *group(*first),
        *group(*second),
    )
    return mixed, one.reshape(first[-1].shape), two.reshape(second[-1].shape)


def unpacked(lengths, tokens, first, second):
    batch_size, head_count, key_dim, value_dim = first[-1].shape
    slots = tokens.shape[0]
    block_len = slots // batch_size
    table = jnp.tile(rope_tables(block_len, key_dim), (batch_size, 1))
    x, states = tokens, []
    for gain, query, key, value, gate, out, state in (first, second):
        qk = []
        for weight in (query, key):
            qk.append(weight.reshape(weight.shape[0], head_count, key_dim))
        x, new_state = plain_block(x, lengths, gain, qk, value, gate, out, state, table)
        states.append(new_state)
    return (x, *states)


def shards(
    tokens,
    lengths,
    gain_first,
    query_first,
    key_first,
    value_first,
    gate_first,
    out_first,
    state_first,
    gain_second,
    query_second,
    key_second,
    value_second,
    gate_second,
    out_second,
    state_second,
):
    n = lax.axis_size("tp")
    batch_size, head_count, key_dim, value_dim = state_first.shape
    slots, width = tokens.shape
    block_len = slots // batch_size
    rows = LIVE_TOTAL
    lengths = lengths.astype(jnp.int32)
    first = (gain_first, query_first, key_first, value_first, gate_first, out_first, state_first)
    second = (gain_second, query_second, key_second, value_second, gate_second, out_second, state_second)
    pieces = next((p for p in (10, 8, 6, 4) if rows % (16 * p) == 0 and rows // p <= 128 - FRONT), 0)
    fits = (
        n >= 8
        and n % 2 == 0
        and pieces > 0
        and head_count == 1
        and width == 128
        and value_dim == 128
        and key_dim == 64
        and block_len <= FRONT
        and 128 % (2 * block_len) == 0
        and 3 * block_len <= 128
        and batch_size <= 128
        and batch_size % 2 == 0
        and slots % 128 == 0
    )
    if not fits:
        return unpacked(lengths, tokens, first, second)
    plan = Plan(n, rows, pieces, batch_size, block_len, key_dim, value_dim, width)
    return fused(plan, n * head_count, lengths, tokens, first, second)


def solution(mesh):
    heads = P(None, "tp")
    state = P("grp", "tp", None, None)
    block = (P(), heads, heads, heads, heads, P("tp", None), state)
    in_specs = (P("grp", "tp"), P("grp")) + block + block
    out_specs = (P("grp", "tp"), state, state)
    return jax.shard_map(shards, mesh=mesh, in_specs=in_specs, out_specs=out_specs, check_vma=False)
```

time: 166 us -> 131 us (0.79)
  Pallas kernels: 148 us -> 123 us
  matrix products: 9.43 us -> 0 us
  other arithmetic: 4.61 us -> 0 us
  local copies, waits for them, and re-layouts: 3.32 us -> 7.55 us
    pallas_call x5 -> x1, Pallas kernels: 148 us -> 123 us  [fused(): pl.pallas_call(functools.partial(whole_kernel, plan), out_shape=[jax.Shap...]
    dot_general x4 -> x0, matrix products: 9.43 us -> none  [the longest x2 3.88 us: packed(): return jnp.dot(pack, padded, preferred_element_type=F32)]
    unnamed x2 -> x5, local copies, waits for them, and re-layouts: 0.01 us -> 7.55 us
    another operation x4 -> x0, local copies, waits for them, and re-layouts: 2.09 us -> none  [the longest x2 1.29 us: shards(): jnp.stack([target.astype(F32), inward.reshape(slots), onward.reshape(slot...]
    sub x2 -> x0, other arithmetic: 1.84 us -> none  [the longest x1 1.17 us: shards(): gap = jnp.maximum(count[:, None] - 1.0 - slot_f[None, :], 0.0)]
where the time goes in v1:
time: 131 us
  Pallas kernels  123 us (94%)
  local copies, waits for them, and re-layouts  7.55 us (6%)
    pallas_call x1, Pallas kernels, fused(): pl.pallas_call(functools.partial(whole_kernel, plan), out_shape=[jax.Shap...  123 us
    unnamed x5, local copies, waits for them, and re-layouts  7.55 us

profile of v1, /device:TPU:0, one launch (start us, length us, event | category | flops | bytes accessed | tf_op | source)
XLA Modules:
  0.0 131.0 jit_solution(10386250317238574247)
XLA Ops:
  0.6 122.8 %shard_map.202 = (bf16[1536,128]{1,0:T(8,128)(2,1)}, f32[96,64,128]{2,1,0:T(8,128)}, f32[96,64,128]{2,1,0:T(8,128)}) custom-call(s32[96]{0:T(128)} %refs_0_.1, f32[16,17]{1,0:T(8,128)} %constant.6.clone.refs_1_, f32[1,16]{1,0:T(1,128)} %constant.7.clone.refs_2_, s32[1,96]{1,0:T(1,128)} %bitcast.25, bf16[1536,128]{1,0:T(8,128)(2,1)} %refs_4_.1, ...), custom_call_target="tpu_custom_call" | custom-call | tf_op jit(solution)/shard_map/pallas_call | solution.py:791
  123.5 1.8 %copy.27 = bf16[1536,128]{1,0:T(8,128)(2,1)} copy(bf16[1536,128]{1,0:T(8,128)(2,1)} %get-tuple-element.15) | data formatting | bytes 786432
  125.2 0.0 copy-start
  125.2 4.1 %copy.28 = f32[96,1,64,128]{3,2,1,0:T(8,128)} copy(f32[96,1,64,128]{3,2,1,0:T(8,128)} %bitcast.16) | data formatting | bytes 6291456
  129.3 0.0 copy-done
  129.3 1.7 %copy.29 = f32[96,1,64,128]{3,2,1,0:T(8,128)} copy(f32[96,1,64,128]{3,2,1,0:T(8,128)S(1)} %bitcast.15) | data formatting | bytes 6291456
Async XLA Ops:
  125.2 4.1 %copy-start = (f32[96,64,128]{2,1,0:T(8,128)S(1)}, f32[96,64,128]{2,1,0:T(8,128)}, u32[]{:S(2)}) copy-start(f32[96,64,128]{2,1,0:T(8,128)} %get-tuple-element.8) | copy-start | bytes 9437188

commit v2 on v1

--- a/solution.py
+++ b/solution.py
@@ -110,7 +110,7 @@
 
 class Plan:
     def __init__(self, n, rows, pieces, batch, block_len, key_dim, value_dim, width):
-        self.n, self.m = n, n // 2
+        self.n, self.m, self.far = n, n // 2, n // 4
         self.rows, self.pieces, self.size = rows, pieces, rows // pieces
         self.batch, self.block_len = batch, block_len
         self.key_dim, self.value_dim, self.width = key_dim, value_dim, width
@@ -119,14 +119,10 @@
         self.units = self.slots // self.unit
         self.group = self.unit // block_len
         self.long = -(-(rows + FRONT) // 128) * 128
-        half, quarter = pieces // 2, pieces // 4
-        self.cw = [j for j in range(pieces) if j < quarter or j >= quarter + half]
-        self.ccw = [j for j in range(pieces) if quarter <= j < quarter + half]
-        self.blocks = [(0, quarter), (quarter, half), (half, quarter + half), (quarter + half, pieces)]
-        self.order = [j for pair in zip(self.cw, self.ccw) for j in pair]
-
-    def clockwise(self, j):
-        return j in self.cw
+        self.blocks = [(j, j + 2) for j in range(0, pieces, 2)]
+
+    def reach(self, j, way):
+        return self.far if j % 2 == way else self.far - 1
 
     def piece(self, j):
         return pl.ds(j * self.size, self.size)
@@ -152,30 +148,28 @@
         self.pos = (1 - odd) * half + odd * (self.m - 1 - half)
         self.me = me
         self.partner = chip * 2 + 1 - self.core
-        self.right = self.device(self.pos + 1)
-        self.left = self.device(self.pos - 1)
+        self.next = (self.device(self.pos + 1), self.device(self.pos - 1))
 
     def device(self, pos):
         m = self.m
         pos = lax.rem(pos + m, m)
-        far = lax.div(pos, (m + 1) // 2)
+        far = lax.div(pos, m // 2)
         chip = (1 - far) * 2 * pos + far * (2 * (m - 1 - pos) + 1)
         return chip * 2 + self.core
 
     def greet(self):
         barrier = pltpu.get_barrier_semaphore()
-        for device in (self.left, self.right, self.partner):
+        for device in (*self.next, self.partner):
             pl.semaphore_signal(barrier, inc=1, device_id={"tp": device}, device_id_type=MESH)
 
     def met(self):
         pl.semaphore_wait(pltpu.get_barrier_semaphore(), 3)
 
-    def to(self, j):
-        return self.right if self.plan.clockwise(j) else self.left
-
-    def origin(self, j, steps):
-        back = self.pos - steps if self.plan.clockwise(j) else self.pos + steps
-        return self.device(back)
+    def behind(self, way, steps):
+        return self.device(self.pos - steps if way == 0 else self.pos + steps)
+
+    def ahead(self, way, steps):
+        return self.device(self.pos + steps if way == 0 else self.pos - steps)
 
 
 def remote(src, dst, send, recv, device):
@@ -189,70 +183,62 @@
     )
 
 
-def share_out(step, steps, total, work):
-    per = -(-total // steps)
-    for k in range(per):
-        u = (step - 1) * per + k
-
-        @pl.when(u < total)
-        def _():
-            work(u)
-
-
 class Gather:
     def __init__(self, ring, own, whole, sems):
         self.ring, self.plan, self.own, self.whole = ring, ring.plan, own, whole
-        self.send, self.recv, self.share_send, self.share_recv = sems
+        self.out, self.recv, self.share_recv = sems
 
     def columns(self, device):
         return pl.ds(pl.multiple_of(device * self.plan.width, self.plan.width), self.plan.width)
 
-    def place(self, j, s):
-        return self.whole.at[self.plan.piece(j), self.columns(self.ring.origin(j, s))]
-
-    def source(self, j, s):
-        if isinstance(s, int) and s == 0:
-            return self.own.at[self.plan.piece(j), :]
-        return self.place(j, s)
-
-    def hop(self, j, s):
+    def place(self, j, way, h):
+        return self.whole.at[self.plan.piece(j), self.columns(self.ring.behind(way, h))]
+
+    def source(self, j, way, h):
+        return self.own.at[self.plan.piece(j), :] if h == 0 else self.place(j, way, h)
+
+    def hop(self, j, way, h):
         return remote(
-            self.source(j, s), self.place(j, s), self.send.at[j, s], self.recv.at[j, s], self.ring.to(j)
+            self.source(j, way, h - 1),
+            self.place(j, way, h - 1),
+            self.out.at[0],
+            self.recv.at[j, way, h - 1],
+            self.ring.next[way],
         )
 
-    def share(self, j, s):
+    def share(self, j, way, h):
         return remote(
-            self.source(j, s),
-            self.place(j, s),
-            self.share_send.at[j, s],
-            self.share_recv.at[j, s],
+            self.source(j, way, h),
+            self.place(j, way, h),
+            self.out.at[1],
+            self.share_recv.at[j // 2, h],
             self.ring.partner,
         )
 
     def begin(self, j):
-        self.hop(j, 0).start()
-        self.share(j, 0).start()
+        for way in (0, 1):
+            self.hop(j, way, 1).start()
+        self.share(j, 0, 0).start()
         self.whole[self.plan.piece(j), self.columns(self.ring.me)] = self.own[self.plan.piece(j), :]
 
-    def forward(self, j, s, last):
-        self.hop(j, s - 1).wait_recv()
-        if not last:
-            self.hop(j, s).start()
-        self.share(j, s).start()
+    def arrive(self, j, way, h):
+        reach = self.plan.reach(j, way)
+        if h > reach:
+            return
+        self.hop(j, way, h).wait_recv()
+        if h < reach:
+            self.hop(j, way, h + 1).start()
+        self.share(j, way, h).start()
+
+    def shared(self, k, h):
+        wide = self.plan.width if h in (0, self.plan.far) else 2 * self.plan.width
+        every = self.whole.at[self.plan.span(self.plan.blocks[k]), pl.ds(0, wide)]
+        remote(every, every, self.out.at[1], self.share_recv.at[k, h], self.ring.partner).wait_recv()
 
     def drain(self):
-        for j in range(self.plan.pieces):
-            self.hop(j, 0).wait_send()
-            self.share(j, 0).wait_send()
-
-        @pl.loop(1, self.plan.m - 1)
-        def _(s):
-            for j in range(self.plan.pieces):
-                self.hop(j, s).wait_send()
-                self.share(j, s).wait_send()
-
-        for j in range(self.plan.pieces):
-            self.share(j, self.plan.m - 1).wait_send()
+        for k, count in enumerate((self.plan.m - 1, self.plan.m)):
+            every = self.whole.at[:, pl.ds(0, count * self.plan.width)]
+            remote(every, every, self.out.at[k], self.share_recv.at[0, 0], self.ring.partner).wait_send()
 
 
 class Projection:
@@ -260,34 +246,38 @@
         self.gather, self.plan, self.ring = gather, gather.plan, gather.ring
         self.gain, self.wcat, self.total, self.squares = gain, wcat, total, squares
 
-    def product(self, block, s):
+    def product(self, at, h):
         plan = self.plan
-        for j in range(*block):
-            self.gather.share(j, s).wait_recv()
-        chip = lax.div(self.ring.origin(block[0], s), 2)
-        cols = pl.ds(pl.multiple_of(chip * 2 * plan.width, 2 * plan.width), 2 * plan.width)
-        x = self.gather.whole[plan.span(block), cols].astype(F32)
-        square = x * x
-        part = square[:, :128]
-        for k in range(128, 2 * plan.width, 128):
-            part = part + square[:, k : k + 128]
-        scaled = (x * self.gain[:, cols]).astype(BF16)
-        return jnp.dot(scaled, self.wcat[cols, :], preferred_element_type=F32), part
-
-    def first(self, block):
-        at = self.plan.span(block)
-        self.total[at, :], self.squares[at, :] = self.product(block, 0)
-
-    def add(self, block, s):
-        at = self.plan.span(block)
-        product, part = self.product(block, s)
-        self.total[at, :] += product
-        self.squares[at, :] += part
+        product, part = None, None
+        for way in (0, 1) if 0 < h < plan.far else (0,):
+            chip = lax.div(self.ring.behind(way, h), 2)
+            cols = pl.ds(pl.multiple_of(chip * 2 * plan.width, 2 * plan.width), 2 * plan.width)
+            x = self.gather.whole[at, cols].astype(F32)
+            square = x * x
+            for k in range(0, 2 * plan.width, 128):
+                part = square[:, k : k + 128] if part is None else part + square[:, k : k + 128]
+            scaled = (x * self.gain[:, cols]).astype(BF16)
+            term = jnp.dot(scaled, self.wcat[cols, :], preferred_element_type=F32)
+            product = term if product is None else product + term
+        return product, part
+
+    def add(self, k, h):
+        plan = self.plan
+        block = plan.blocks[k]
+        self.gather.shared(k, h)
+        at = plan.span(block)
+        product, part = self.product(at, h)
+        if h == 0:
+            self.total[at, :], self.squares[at, :] = product, part
+        else:
+            self.total[at, :] += product
+            self.squares[at, :] += part
 
     def finish(self, block, table, queries, kv, gate):
         plan = self.plan
         at = plan.span(block)
-        product, part = self.product(block, plan.m - 1)
+        self.gather.shared(plan.blocks.index(block), plan.far)
+        product, part = self.product(at, plan.far)
         square = self.squares[at, :] + part
         mean = jnp.sum(square, axis=-1, keepdims=True) / (plan.n * plan.width)
         out = (self.total[at, :] + product) * lax.rsqrt(mean + NORM_EPSILON)
@@ -331,7 +321,7 @@
     bounds[0:8, :] = begin
     bounds[8:16, :] = begin + lens.astype(F32)
     base = lax.broadcasted_iota(jnp.int32, (plan.size, plan.slots), 0).astype(F32)
-    for j in plan.order:
+    for j in range(plan.pieces):
         hot = jnp.where(base + float(j * plan.size) == trow[0:1, :], 1.0, 0.0).astype(BF16)
         x[plan.piece(j), :] = jnp.dot(hot, tokens[...], preferred_element_type=F32).astype(BF16)
         send(j)
@@ -394,17 +384,18 @@
     values = padded[:, both:].astype(BF16)
     scaled = padded[:, :both] * onward[at, :]
     high = scaled.astype(BF16).astype(F32)
-    wide = (plan.unit, plan.group * plan.key_dim)
-    own = lax.div(lax.broadcasted_iota(jnp.int32, wide, 0), plan.block_len) == lax.div(
-        lax.broadcasted_iota(jnp.int32, wide, 1), plan.key_dim
+    stacked = jnp.concatenate([high, scaled - high], axis=0)
+    wide = (2 * plan.unit, plan.group * plan.key_dim)
+    own = lax.rem(
+        lax.div(lax.broadcasted_iota(jnp.int32, wide, 0), plan.block_len), plan.group
+    ) == lax.div(lax.broadcasted_iota(jnp.int32, wide, 1), plan.key_dim)
+    spread = jnp.where(own, jnp.concatenate([stacked] * (plan.group // 2), axis=1), 0.0)
+    added = lax.dot_general(
+        spread.astype(BF16),
+        jnp.concatenate([values, values], axis=0),
+        (((0,), (0,)), ((), ())),
+        preferred_element_type=F32,
     )
-    added = None
-    for piece in (high, scaled - high):
-        spread = jnp.where(own, jnp.concatenate([piece] * (plan.group // 2), axis=1), 0.0)
-        term = lax.dot_general(
-            spread.astype(BF16), values, (((0,), (0,)), ((), ())), preferred_element_type=F32
-        )
-        added = term if added is None else added + term
     for b in range(plan.group):
         which = u * plan.group + b
         decay = powers[me, lens_smem[which]]
@@ -435,11 +426,15 @@
     pick = owner - jnp.where(lane < plan.key_dim, 0.0, 1.0).astype(BF16)
     zero = jnp.zeros_like(q)
     spread = [jnp.where(pick == jnp.asarray(2.0 * c, BF16), q, zero) for c in range(low, high)]
-    carried = jnp.dot(
-        jnp.concatenate(spread, axis=1),
-        halves[low * both : high * both, :],
-        preferred_element_type=F32,
-    )
+    middle = (low + high) // 2
+    carried = None
+    for first, last in ((low, middle), (middle, high)):
+        term = jnp.dot(
+            jnp.concatenate(spread[first - low : last - low], axis=1),
+            halves[first * both : last * both, :],
+            preferred_element_type=F32,
+        )
+        carried = term if carried is None else carried + term
     carried = carried[:, : plan.value_dim] + carried[:, plan.value_dim :]
     retained = jnp.concatenate(inner, axis=0) + carried * jnp.exp(rate * (tcol[at, :] + 1.0))
     inv = lax.rsqrt(jnp.mean(retained * retained, axis=-1, keepdims=True) + NORM_EPSILON)
@@ -450,84 +445,92 @@
     def __init__(self, ring, h_pair, w_pair, outbox, inbox, parts, sems):
         self.ring, self.plan = ring, ring.plan
         self.h_pair, self.w_pair, self.outbox, self.inbox, self.parts = h_pair, w_pair, outbox, inbox, parts
-        self.send, self.recv, self.pair_send, self.pair_recv = sems
+        self.out, self.recv, self.pair_recv = sems
 
     def offer(self, k):
         rows, depth = self.plan.span(self.plan.blocks[k]), self.plan.value_dim
         return remote(
             self.h_pair.at[rows, pl.ds(0, depth)],
             self.h_pair.at[rows, pl.ds(depth, depth)],
-            self.pair_send.at[k],
+            self.out.at[1],
             self.pair_recv.at[k],
             self.ring.partner,
         )
 
-    def hop(self, j, s):
+    def hop(self, j, way, i):
         return remote(
-            self.outbox.at[j, s],
-            self.inbox.at[j, s],
-            self.send.at[j, s],
-            self.recv.at[j, s],
-            self.ring.to(j),
+            self.outbox.at[j, way, i - 1],
+            self.inbox.at[j, way, i - 1],
+            self.out.at[0],
+            self.recv.at[j, way, i - 1],
+            self.ring.next[way],
         )
 
-    def product(self, k, s):
-        block, width = self.plan.blocks[k], self.plan.width
-        target = self.ring.origin(block[0], s + 1)
-        cols = pl.ds(pl.multiple_of(target * width, width), width)
-        return jnp.dot(
-            self.h_pair[self.plan.span(block), :], self.w_pair[:, cols], preferred_element_type=F32
+    def prepare(self, k, distance):
+        plan = self.plan
+        ways = (0, 1) if 0 < distance < plan.far else (0,)
+        at = plan.span(plan.blocks[k])
+        columns = []
+        for way in ways:
+            target = self.ring.ahead(way, distance)
+            columns.append(self.w_pair[:, pl.ds(pl.multiple_of(target * plan.width, plan.width), plan.width)])
+        part = jnp.dot(
+            self.h_pair[at, :], jnp.concatenate(columns, axis=1), preferred_element_type=F32
         )
+        for way in ways:
+            self.parts[way, distance % 2, at, :] = part[:, way * plan.width : (way + 1) * plan.width]
 
     def begin(self, k):
+        plan = self.plan
         self.offer(k).wait_recv()
-        part = self.product(k, 0).astype(BF16)
-        first, last = self.plan.blocks[k]
-        for j in range(first, last):
-            self.outbox[j, 0] = part[(j - first) * self.plan.size : (j - first + 1) * self.plan.size, :]
-            self.hop(j, 0).start()
-
-    def prepare(self, k, s):
-        self.parts[lax.rem(s, 2), self.plan.span(self.plan.blocks[k]), :] = self.product(k, s)
-
-    def take(self, j, s):
-        self.hop(j, s - 1).wait_recv()
-        return self.parts[lax.rem(s, 2), self.plan.piece(j), :] + self.inbox[j, s - 1].astype(F32)
-
-    def forward(self, j, s):
-        self.outbox[j, s] = self.take(j, s).astype(BF16)
-        self.hop(j, s).start()
-
-    def steps(self, work):
-        for k in range(4):
-            self.prepare(k, 1)
-
-        @pl.loop(1, self.plan.m - 1)
-        def _(s):
-            for i, j in enumerate(self.plan.order):
-                self.forward(j, s)
-                if i % 2 == 1 and i < 8:
-                    self.prepare(i // 2, s + 1)
-            for i in range(len(self.plan.order) // 2, 4):
-                self.prepare(i, s + 1)
-            work(s)
+        self.prepare(k, plan.far)
+        for j in range(*plan.blocks[k]):
+            way = j % 2
+            self.outbox[j, way, 0] = self.parts[0, plan.far % 2, plan.piece(j), :].astype(BF16)
+            self.hop(j, way, 1).start()
+        self.prepare(k, plan.far - 1)
+        for j in range(*plan.blocks[k]):
+            way = 1 - j % 2
+            self.outbox[j, way, 0] = self.parts[way, (plan.far - 1) % 2, plan.piece(j), :].astype(BF16)
+            self.hop(j, way, 1).start()
+        self.prepare(k, plan.far - 2)
+
+    def arrive(self, j, way, i):
+        distance = self.plan.reach(j, way) - i
+        if distance <= 0:
+            return
+        self.hop(j, way, i).wait_recv()
+        part = self.parts[way, distance % 2, self.plan.piece(j), :] + self.inbox[j, way, i - 1].astype(F32)
+        self.outbox[j, way, i] = part.astype(BF16)
+        self.hop(j, way, i + 1).start()
+
+    def round(self, k, i):
+        plan = self.plan
+        for j in range(*plan.blocks[k]):
+            for way in (0, 1):
+                self.arrive(j, way, i)
+        if plan.far - 2 - i >= 0:
+            self.prepare(k, plan.far - 2 - i)
 
     def last(self, j):
-        return self.take(j, self.plan.m - 1).astype(BF16).astype(F32)
-
-    def drain(self):
-        for k in range(4):
-            self.offer(k).wait_send()
-
-        @pl.loop(0, self.plan.m - 1)
-        def _(s):
-            for j in range(self.plan.pieces):
-                self.hop(j, s).wait_send()
+        plan = self.plan
+        total = self.parts[0, 0, plan.piece(j), :]
+        for way in (1 - j % 2, j % 2):
+            reach = plan.reach(j, way)
+            self.hop(j, way, reach).wait_recv()
+            total = total + self.inbox[j, way, reach - 1].astype(F32)
+        return total.astype(BF16).astype(F32)
+
+    def drain(self, whole):
+        every = whole.at[:, pl.ds(0, (self.plan.m - 1) * self.plan.width)]
+        remote(every, every, self.out.at[0], self.pair_recv.at[0], self.ring.partner).wait_send()
+        half = self.h_pair.at[:, pl.ds(0, self.plan.value_dim)]
+        remote(half, half, self.out.at[1], self.pair_recv.at[0], self.ring.partner).wait_send()
 
 
 def whole_kernel(plan, *refs):
     (lens_smem, powers, rates, lens_ref, tokens, rope, *rest) = refs
-    gains, raw, outs_w, states_in, (mixed, *states_out), scratch = (
+    gains, raw, outs_w, states_in, (mixed, *states), scratch = (
         (rest[0], rest[7]),
         (rest[1:5], rest[8:12]),
         (rest[5], rest[12]),
@@ -536,9 +539,9 @@
         rest[17:],
     )
     (x, x1, y, whole, wcats, turned, w_pairs, total, squares, table, gate, tcol, bcol, queries) = scratch[:14]
-    (kv, halves, states, hot, onward, tgt, parts, outbox, inbox, h_pair, trow, bounds, fade) = scratch[14:27]
-    load, store, pair_w = scratch[27:30]
-    sems = scratch[30:]
+    (kv, halves, hot, onward, tgt, parts, outbox, inbox, h_pair, trow, bounds, fade) = scratch[14:26]
+    load, pair_w = scratch[26:28]
+    sems = scratch[28:]
     ring = Ring(plan)
     ring.greet()
     depth, both = plan.value_dim, 2 * plan.key_dim
@@ -553,7 +556,7 @@
             (wv, wcats.at[i, :, pl.ds(both, depth)]),
             (wg, wcats.at[i, :, pl.ds(both + depth, depth)]),
             (outs_w[i], w_pairs.at[i, pl.ds(0, depth), :]),
-            (states_in[i], states.at[i]),
+            (states_in[i], states[i]),
         )
         for k, (source, target) in enumerate(targets):
             loads[i, k] = pltpu.make_async_copy(source, target, load.at[i, k])
@@ -567,9 +570,9 @@
             ring.partner,
         )
 
-    gathers = [Gather(ring, (x, x1)[i], whole, sems[8 * i : 8 * i + 4]) for i in range(2)]
+    gathers = [Gather(ring, (x, x1)[i], whole, sems[:3]) for i in range(2)]
     scatters = [
-        Scatter(ring, h_pair, w_pairs.at[i], outbox, inbox, parts, sems[8 * i + 4 : 8 * i + 8])
+        Scatter(ring, h_pair, w_pairs.at[i], outbox, inbox, parts, sems[3:])
         for i in range(2)
     ]
     projections = [Projection(gathers[i], gains[i], wcats.at[i], total, squares) for i in range(2)]
@@ -609,103 +612,116 @@
     loads[0, 4].wait()
     swap(0).start()
 
-    def run(i, gather_work, before_last, scatter_work, finish):
+    def run(i, gather_work, scatter_work, finish):
         gather, projection, scatter = gathers[i], projections[i], scatters[i]
-        m, blocks = plan.m, plan.blocks
-
-        def gather_step(s, last):
-            for k, j in enumerate(plan.order):
-                gather.forward(j, s, last)
-                if k % 2 == 1 and k < 8:
-                    if isinstance(s, int) and s == 1:
-                        projection.first(blocks[k // 2])
-                    else:
-                        projection.add(blocks[k // 2], s - 1)
-            for k in range(len(plan.order) // 2, 4):
-                if isinstance(s, int) and s == 1:
-                    projection.first(blocks[k])
-                else:
-                    projection.add(blocks[k], s - 1)
-
-        gather_step(1, False)
-        gather_work(1)
-
-        @pl.loop(2, m - 1)
-        def _(s):
-            gather_step(s, False)
-            gather_work(s)
-
-        gather_step(m - 1, True)
-        before_last()
-        gather.drain()
-
-        def retain_block(k):
-            block = blocks[k]
-            projection.finish(block, table, queries, kv, gate)
-            h_pair[plan.span(block), :depth] = retention_block(
-                plan, rate, block, queries, kv, gate, tcol, bcol, fade, halves
+        far, blocks = plan.far, plan.blocks
+
+        def step(k, h):
+            for j in range(*blocks[k]):
+                for way in (0, 1):
+                    gather.arrive(j, way, h)
+            projection.add(k, h - 1)
+            if gather_work:
+                gather_work.pop(0)()
+
+        for h in range(1, far):
+            for k in range(len(blocks)):
+                step(k, h)
+
+        def project(k):
+            projection.finish(blocks[k], table, queries, kv, gate)
+
+        def retain(k):
+            h_pair[plan.span(blocks[k]), :depth] = retention_block(
+                plan, rate, blocks[k], queries, kv, gate, tcol, bcol, fade, halves
             )
             scatter.offer(k).start()
 
-        retain_block(0)
-        retain_block(1)
-        swap(i).wait_recv()
-        scatter.begin(0)
-        retain_block(2)
-        scatter.begin(1)
-        retain_block(3)
-        scatter.begin(2)
-        scatter.begin(3)
-        scatter.steps(scatter_work)
-        for j in plan.order:
+        def round(k, r):
+            scatter.round(k, r)
+            if r > 1 and scatter_work:
+                scatter_work.pop(0)()
+
+        many = len(blocks)
+        ahead = 3
+        for k in range(min(ahead, many)):
+            step(k, far)
+        for k in range(many):
+            project(k)
+            retain(k)
+            if k + ahead < many:
+                step(k + ahead, far)
+            elif gather_work:
+                while gather_work:
+                    gather_work.pop(0)()
+            if k == 0:
+                swap(i).wait_recv()
+            else:
+                scatter.begin(k - 1)
+            if k >= 3:
+                round(k - 3, 1)
+        gather.drain()
+        round(many - 3, 1)
+        scatter.begin(many - 1)
+        for k in (many - 2, many - 1):
+            round(k, 1)
+        for r in range(2, far):
+            for k in range(many):
+                round(k, r)
+        while scatter_work:
+            scatter_work.pop(0)()
+        for j in range(plan.pieces):
             finish(j, scatter.last(j))
-        scatter.drain()
-        swap(i).wait_send()
-
-    def first_gather(s):
-        share_out(s, plan.m - 2, plan.pieces, lambda u: row_unit(plan, bounds, rope, tcol, bcol, table, u))
-        share_out(s, plan.m - 2, plan.units, lambda u: split_unit(plan, states.at[0], halves, u))
-        share_out(
-            s, plan.m - 2, plan.units, lambda u: slot_unit(plan, rate, lens_ref, tgt, onward, hot, u)
-        )
-
-    def update(i, s):
-        share_out(
-            s,
-            plan.m - 2,
-            plan.units,
-            lambda u: state_unit(plan, lens_smem, powers, ring.me, hot, kv, onward, states.at[i], u),
-        )
-
-    def first_scatter(s):
-        update(0, s)
+
+    def every(first, last, unit_work):
+        def act():
+            @pl.loop(first, last)
+            def _(u):
+                unit_work(u)
+
+        return act
+
+    units = plan.units
+
+    def update(i, times):
+        body = lambda u: state_unit(plan, lens_smem, powers, ring.me, hot, kv, onward, states[i], u)
+        return spread_out(units, times, body)
+
+    def halve(i):
+        return every(0, units, lambda u: split_unit(plan, states[i], halves, u))
+
+    slot_body = lambda u: slot_unit(plan, rate, lens_ref, tgt, onward, hot, u)
+    row_body = lambda u: row_unit(plan, bounds, rope, tcol, bcol, table, u)
+    spread_out = lambda total, times, body: [
+        every(total * k // times, total * (k + 1) // times, body) for k in range(times)
+    ]
+    first_work = spread_out(plan.pieces, 2, row_body) + [halve(0)] + spread_out(units, 4, slot_body)
 
     def after_first(j, mix):
         at = plan.piece(j)
         x1[at, :] = (x[at, :].astype(F32) + mix).astype(BF16)
         gathers[1].begin(j)
 
-    run(0, first_gather, lambda: None, first_scatter, after_first)
-    save = pltpu.make_async_copy(states.at[0], states_out[0], store.at[0])
-    save.start()
-    for k in range(6):
-        loads[1, k].wait()
-    swap(1).start()
-
-    @pl.loop(0, wcats.shape[1] // 128)
-    def _(u):
-        fill_unit(turned.at[1, 0], turned.at[1, 1], wcats.at[1], u)
-
-    def second_gather(s):
-        share_out(s, plan.m - 2, plan.units, lambda u: split_unit(plan, states.at[1], halves, u))
+    def ready_second():
+        for k in range(6):
+            loads[1, k].wait()
+        swap(1).start()
+
+        @pl.loop(0, wcats.shape[1] // 128)
+        def _(u):
+            fill_unit(turned.at[1, 0], turned.at[1, 1], wcats.at[1], u)
+
+    run(0, first_work, [ready_second], after_first)
+    scatters[0].drain(whole)
+    swap(0).wait_send()
 
     def after_second(j, mix):
         at = plan.piece(j)
         y[pl.ds(FRONT + j * plan.size, plan.size), :] = (x1[at, :].astype(F32) + mix).astype(BF16)
 
-    run(1, second_gather, lambda: None, lambda s: update(1, s), after_second)
-    save_second = pltpu.make_async_copy(states.at[1], states_out[1], store.at[1])
-    save_second.start()
+    run(1, [halve(1)] + update(0, 6), update(1, 6), after_second)
+    scatters[1].drain(whole)
+    swap(1).wait_send()
     many = next(k for k in (3, 2, 1) if plan.units % k == 0)
 
     @pl.loop(0, plan.units // many)
@@ -714,9 +730,6 @@
         spread = jnp.dot(hot[at, :], y[...], preferred_element_type=F32)
         live = jnp.concatenate([tgt[at, :]] * (plan.width // 128), axis=1) >= 0.0
         mixed[at, :] = jnp.where(live, spread, tokens[at, :].astype(F32)).astype(BF16)
-
-    save.wait()
-    save_second.wait()
 
 
 def fused(plan, heads, lengths, tokens, first, second):
@@ -739,7 +752,7 @@
     rope = np.zeros((128, rope.shape[1]), jnp.bfloat16)
     rope[: 3 * plan.block_len] = np.concatenate(stacked, axis=0)
 
-    n, m, rows, width = plan.n, plan.m, plan.rows, plan.width
+    n, rows, width = plan.n, plan.rows, plan.width
     wide, both = 2 * plan.key_dim + 2 * plan.value_dim, 2 * plan.key_dim
     depth = plan.value_dim
     model = n * width
@@ -763,43 +776,45 @@
         vmem((rows, both), BF16),
         vmem((plan.long, both + depth), BF16),
         vmem((plan.batch * plan.key_dim, 2 * depth), BF16),
-        vmem((2,) + state_shape, F32),
         vmem((plan.slots, plan.long), BF16),
         vmem((plan.slots, 128), F32),
         vmem((plan.slots, 128), F32),
-        vmem((2, rows, width), F32),
-        vmem((plan.pieces, m - 1, plan.size, width), BF16),
-        vmem((plan.pieces, m - 1, plan.size, width), BF16),
+        vmem((2, 2, rows, width), F32),
+        vmem((plan.pieces, 2, plan.far, plan.size, width), BF16),
+        vmem((plan.pieces, 2, plan.far, plan.size, width), BF16),
         vmem((rows, 2 * depth), BF16),
         vmem((8, plan.slots), F32),
         vmem((16, plan.batch), F32),
         vmem((plan.size, 128), F32),
         dma(2, 6),
-        dma(2),
         dma(2, 2),
     ]
-    for _ in range(2):
-        scratch += [dma(plan.pieces, m - 1)] * 2 + [dma(plan.pieces, m)] * 2
-        scratch += [dma(plan.pieces, m - 1)] * 2 + [dma(4)] * 2
+    scratch += [dma(2), dma(plan.pieces, 2, plan.far), dma(len(plan.blocks), plan.far + 1)]
+    scratch += [dma(2), dma(plan.pieces, 2, plan.far), dma(len(plan.blocks))]
     spec = lambda space: pl.BlockSpec(memory_space=space)
     inside, outside, scalars = spec(pltpu.VMEM), spec(pltpu.HBM), spec(pltpu.SMEM)
 
     def group(gain, query, key, value, gate, out, state):
-        return (gain[None], query.T, key.T, value, gate, out, state.reshape(state_shape))
+        far = [
+            pltpu.with_memory_space_constraint(a, pltpu.HBM)
+            for a in (query.T, key.T, value, gate, out, state.reshape(state_shape))
+        ]
+        return (gain[None], *far)
 
     block_specs = [inside] + [outside] * 6
+
     mixed, one, two = pl.pallas_call(
         functools.partial(whole_kernel, plan),
         out_shape=[
-            jax.ShapeDtypeStruct((plan.slots, width), BF16),
-            jax.ShapeDtypeStruct(state_shape, F32),
-            jax.ShapeDtypeStruct(state_shape, F32),
+            pltpu.VMEM((plan.slots, width), BF16),
+            pltpu.VMEM(state_shape, F32),
+            pltpu.VMEM(state_shape, F32),
         ],
         in_specs=[scalars] * 3 + [inside] * 3 + block_specs * 2,
-        out_specs=[inside, outside, outside],
+        out_specs=[inside, inside, inside],
         scratch_shapes=scratch,
         compiler_params=pltpu.CompilerParams(
-            collective_id=0, has_side_effects=True, vmem_limit_bytes=62 * 2**20
+            collective_id=0, has_side_effects=True, vmem_limit_bytes=48 * 2**20
         ),
     )(
         lengths,
@@ -857,9 +872,9 @@
     second = (gain_second, query_second, key_second, value_second, gate_second, out_second, state_second)
     pieces = next((p for p in (10, 8, 6, 4) if rows % (16 * p) == 0 and rows // p <= 128 - FRONT), 0)
     fits = (
-        n >= 8
-        and n % 2 == 0
-        and pieces > 0
+        n >= 12
+        and n % 4 == 0
+        and pieces >= 8
         and head_count == 1
         and width == 128
         and value_dim == 128

time: 131 us -> 108 us (0.82)
  Pallas kernels: 123 us -> 103 us
  local copies, waits for them, and re-layouts: 7.55 us -> 4.08 us
    pallas_call x1, Pallas kernels: 123 us -> 103 us  [fused(): pl.pallas_call(functools.partial(whole_kernel, plan), out_shape=[pltpu.VM...]
    unnamed x5 -> x3, local copies, waits for them, and re-layouts: 7.55 us -> 4.08 us
where the time goes in v2:
time: 108 us
  Pallas kernels  103 us (95%)
  local copies, waits for them, and re-layouts  4.08 us (4%)
    pallas_call x1, Pallas kernels, fused(): pl.pallas_call(functools.partial(whole_kernel, plan), out_shape=[pltpu.VM...  103 us
    unnamed x3, local copies, waits for them, and re-layouts  4.08 us

profile of v2, /device:TPU:0, one launch (start us, length us, event | category | flops | bytes accessed | tf_op | source)
XLA Modules:
  0.0 108.0 jit_solution(12017370887524064389)
XLA Ops:
  0.6 103.3 %shard_map.202 = (bf16[1536,128]{1,0:T(8,128)(2,1)S(1)}, f32[96,64,128]{2,1,0:T(8,128)S(1)}, f32[96,64,128]{2,1,0:T(8,128)S(1)}) custom-call(s32[96]{0:T(128)} %refs_0_.1, f32[16,17]{1,0:T(8,128)} %constant.6.clone.refs_1_, f32[1,16]{1,0:T(1,128)} %constant.7.clone.refs_2_, s32[1,96]{1,0:T(1,128)} %bitcast.25, bf16[1536,128]{1,0:T(8,128)(2,1)} %refs_4_.1, ...), custom_call_target="tpu_custom_call" | custom-call | tf_op jit(solution)/shard_map/pallas_call | solution.py:806
  104.0 0.7 copy.27
  104.7 1.7 %copy.28 = f32[96,1,64,128]{3,2,1,0:T(8,128)} copy(f32[96,1,64,128]{3,2,1,0:T(8,128)S(1)} %bitcast.16) | data formatting | bytes 6291456
  106.4 1.7 %copy.29 = f32[96,1,64,128]{3,2,1,0:T(8,128)} copy(f32[96,1,64,128]{3,2,1,0:T(8,128)S(1)} %bitcast.15) | data formatting | bytes 6291456

commit v3 on v2

--- a/solution.py
+++ b/solution.py
@@ -120,6 +120,9 @@
         self.group = self.unit // block_len
         self.long = -(-(rows + FRONT) // 128) * 128
         self.blocks = [(j, j + 2) for j in range(0, pieces, 2)]
+        lead = -(-3 * len(self.blocks) // 5)
+        self.leading = list(range(lead))
+        self.trailing = list(range(lead, len(self.blocks)))
 
     def reach(self, j, way):
         return self.far if j % 2 == way else self.far - 1
@@ -324,7 +327,8 @@
     for j in range(plan.pieces):
         hot = jnp.where(base + float(j * plan.size) == trow[0:1, :], 1.0, 0.0).astype(BF16)
         x[plan.piece(j), :] = jnp.dot(hot, tokens[...], preferred_element_type=F32).astype(BF16)
-        send(j)
+        if j // 2 in plan.leading:
+            send(j)
 
 
 def row_unit(plan, bounds, rope, tcol, bcol, table, u):
@@ -371,10 +375,7 @@
     at = pl.ds(pl.multiple_of(u * plan.group, plan.group), plan.group)
     rows = plan.group * plan.key_dim
     whole = state[at].reshape(rows, plan.value_dim)
-    high = whole.astype(BF16)
-    to = pl.ds(pl.multiple_of(u * rows, rows), rows)
-    halves[to, : plan.value_dim] = high
-    halves[to, plan.value_dim :] = (whole - high.astype(F32)).astype(BF16)
+    halves[pl.ds(pl.multiple_of(u * rows, rows), rows), :] = whole.astype(BF16)
 
 
 def state_unit(plan, lens_smem, powers, me, hot, kv, onward, state, u):
@@ -435,7 +436,6 @@
             preferred_element_type=F32,
         )
         carried = term if carried is None else carried + term
-    carried = carried[:, : plan.value_dim] + carried[:, plan.value_dim :]
     retained = jnp.concatenate(inner, axis=0) + carried * jnp.exp(rate * (tcol[at, :] + 1.0))
     inv = lax.rsqrt(jnp.mean(retained * retained, axis=-1, keepdims=True) + NORM_EPSILON)
     return (retained * inv * gate[at, :]).astype(BF16)
@@ -593,10 +593,6 @@
     loads[0, 0].wait()
     loads[0, 1].wait()
 
-    @pl.loop(0, wcats.shape[1] // 128)
-    def _(u):
-        fill_unit(turned.at[0, 0], turned.at[0, 1], wcats.at[0], u)
-
     loads[0, 2].wait()
     loads[0, 3].wait()
     shape = (plan.size, 128)
@@ -612,66 +608,80 @@
     loads[0, 4].wait()
     swap(0).start()
 
-    def run(i, gather_work, scatter_work, finish):
-        gather, projection, scatter = gathers[i], projections[i], scatters[i]
-        far, blocks = plan.far, plan.blocks
-
-        def step(k, h):
-            for j in range(*blocks[k]):
+    def step(i, ks, h, work):
+        for k in ks:
+            for j in range(*plan.blocks[k]):
                 for way in (0, 1):
-                    gather.arrive(j, way, h)
-            projection.add(k, h - 1)
-            if gather_work:
-                gather_work.pop(0)()
-
-        for h in range(1, far):
-            for k in range(len(blocks)):
-                step(k, h)
-
-        def project(k):
-            projection.finish(blocks[k], table, queries, kv, gate)
-
-        def retain(k):
-            h_pair[plan.span(blocks[k]), :depth] = retention_block(
-                plan, rate, blocks[k], queries, kv, gate, tcol, bcol, fade, halves
-            )
-            scatter.offer(k).start()
-
-        def round(k, r):
-            scatter.round(k, r)
-            if r > 1 and scatter_work:
-                scatter_work.pop(0)()
-
-        many = len(blocks)
-        ahead = 3
-        for k in range(min(ahead, many)):
-            step(k, far)
-        for k in range(many):
-            project(k)
-            retain(k)
-            if k + ahead < many:
-                step(k + ahead, far)
-            elif gather_work:
-                while gather_work:
-                    gather_work.pop(0)()
-            if k == 0:
-                swap(i).wait_recv()
-            else:
-                scatter.begin(k - 1)
-            if k >= 3:
-                round(k - 3, 1)
-        gather.drain()
-        round(many - 3, 1)
-        scatter.begin(many - 1)
-        for k in (many - 2, many - 1):
-            round(k, 1)
+                    gathers[i].arrive(j, way, h)
+            projections[i].add(k, h - 1)
+            if work:
+                act = work.pop(0)
+                if act:
+                    act()
+
+    def retain(i, k):
+        projections[i].finish(plan.blocks[k], table, queries, kv, gate)
+        h_pair[plan.span(plan.blocks[k]), :depth] = retention_block(
+            plan, rate, plan.blocks[k], queries, kv, gate, tcol, bcol, fade, halves
+        )
+        scatters[i].offer(k).start()
+
+    def turn(i, ks, r, work):
+        for k in ks:
+            scatters[i].round(k, r)
+            if r > (2 if k in leading else 1) and work:
+                work.pop(0)()
+
+    def flush(work):
+        while work:
+            act = work.pop(0)
+            if act:
+                act()
+
+    leading, trailing, far = plan.leading, plan.trailing, plan.far
+
+    def middle(i, h):
+        swapped = False
+        for n, k in enumerate(leading):
+            retain(i, k)
+            if n > 0:
+                if not swapped:
+                    swap(i).wait_recv()
+                    swapped = True
+                scatters[i].begin(leading[n - 1])
+            if h <= far:
+                step(i, trailing, h, [])
+                h += 1
+        while h <= far:
+            step(i, trailing, h, [])
+            h += 1
+        early = list(leading)
+        for n, k in enumerate(trailing):
+            retain(i, k)
+            scatters[i].begin(leading[-1] if n == 0 else trailing[n - 1])
+            turn(i, early[:1], 1, [])
+            early = early[1:]
+        gathers[i].drain()
+        turn(i, early, 1, [])
+        scatters[i].begin(trailing[-1])
+
+    def back(i, work, finish, between):
         for r in range(2, far):
-            for k in range(many):
-                round(k, r)
-        while scatter_work:
-            scatter_work.pop(0)()
-        for j in range(plan.pieces):
-            finish(j, scatter.last(j))
+            behind = list(trailing)
+            for n, k in enumerate(leading):
+                turn(i, [k], r, work)
+                if n > 0 and behind:
+                    turn(i, [behind.pop(0)], r - 1, work)
+            turn(i, behind, r - 1, work)
+        for k in leading:
+            for j in range(*plan.blocks[k]):
+                finish(j, scatters[i].last(j))
+        turn(i, trailing, far - 1, work)
+        flush(work)
+        between()
+        for k in trailing:
+            for j in range(*plan.blocks[k]):
+                finish(j, scatters[i].last(j))
 
     def every(first, last, unit_work):
         def act():
@@ -695,7 +705,8 @@
     spread_out = lambda total, times, body: [
         every(total * k // times, total * (k + 1) // times, body) for k in range(times)
     ]
-    first_work = spread_out(plan.pieces, 2, row_body) + [halve(0)] + spread_out(units, 4, slot_body)
+    rows_work = spread_out(plan.pieces, 2, row_body)
+    first_work = [rows_work[0], None, rows_work[1], None, halve(0)]
 
     def after_first(j, mix):
         at = plan.piece(j)
@@ -711,15 +722,56 @@
         def _(u):
             fill_unit(turned.at[1, 0], turned.at[1, 1], wcats.at[1], u)
 
-    run(0, first_work, [ready_second], after_first)
+    fills = spread_out(
+        wcats.shape[1] // 128,
+        len(leading),
+        lambda u: fill_unit(turned.at[0, 0], turned.at[0, 1], wcats.at[0], u),
+    )
+    for n, k in enumerate(leading):
+        if n > 0:
+            for j in range(*plan.blocks[k]):
+                for way in (0, 1):
+                    gathers[0].arrive(j, way, 1)
+        fills[n]()
+        if n == 0:
+            for j in range(*plan.blocks[k]):
+                for way in (0, 1):
+                    gathers[0].arrive(j, way, 1)
+    for k in trailing:
+        for j in range(*plan.blocks[k]):
+            gathers[0].begin(j)
+    for k in leading:
+        projections[0].add(k, 0)
+    for h in range(2, far):
+        step(0, leading, h, first_work)
+    step(0, trailing, 1, first_work)
+    step(0, leading, far, first_work)
+    flush(first_work)
+    middle(0, 2)
+
+    second_work = []
+    for act in [halve(1)] + update(0, 6):
+        second_work += [act, None]
+    back(
+        0,
+        [ready_second] + spread_out(units, 4, slot_body),
+        after_first,
+        lambda: step(1, leading, 1, []),
+    )
     scatters[0].drain(whole)
     swap(0).wait_send()
+    for h in range(2, far):
+        step(1, leading, h, second_work)
+        step(1, trailing, h - 1, second_work)
+    step(1, leading, far, second_work)
+    flush(second_work)
 
     def after_second(j, mix):
         at = plan.piece(j)
         y[pl.ds(FRONT + j * plan.size, plan.size), :] = (x1[at, :].astype(F32) + mix).astype(BF16)
 
-    run(1, [halve(1)] + update(0, 6), update(1, 6), after_second)
+    middle(1, far - 1)
+    back(1, update(1, 6), after_second, lambda: None)
     scatters[1].drain(whole)
     swap(1).wait_send()
     many = next(k for k in (3, 2, 1) if plan.units % k == 0)
@@ -775,7 +827,7 @@
         vmem((rows, 128), BF16),
         vmem((rows, both), BF16),
         vmem((plan.long, both + depth), BF16),
-        vmem((plan.batch * plan.key_dim, 2 * depth), BF16),
+        vmem((plan.batch * plan.key_dim, depth), BF16),
         vmem((plan.slots, plan.long), BF16),
         vmem((plan.slots, 128), F32),
         vmem((plan.slots, 128), F32),

time: 108 us -> 104 us (0.963)
  Pallas kernels: 103 us -> 99.5 us
    pallas_call x1, Pallas kernels: 103 us -> 99.5 us  [fused(): pl.pallas_call(functools.partial(whole_kernel, plan), out_shape=[pltpu.VM...]
where the time goes in v3:
time: 104 us
  Pallas kernels  99.5 us (96%)
  local copies, waits for them, and re-layouts  4.08 us (4%)
    pallas_call x1, Pallas kernels, fused(): pl.pallas_call(functools.partial(whole_kernel, plan), out_shape=[pltpu.VM...  99.5 us
    unnamed x3, local copies, waits for them, and re-layouts  4.08 us

profile of v3, /device:TPU:0, one launch (start us, length us, event | category | flops | bytes accessed | tf_op | source)
XLA Modules:
  0.0 104.2 jit_solution(18370980955644277843)
XLA Ops:
  0.6 99.5 %shard_map.202 = (bf16[1536,128]{1,0:T(8,128)(2,1)S(1)}, f32[96,64,128]{2,1,0:T(8,128)S(1)}, f32[96,64,128]{2,1,0:T(8,128)S(1)}) custom-call(s32[96]{0:T(128)} %refs_0_.1, f32[16,17]{1,0:T(8,128)} %constant.6.clone.refs_1_, f32[1,16]{1,0:T(1,128)} %constant.7.clone.refs_2_, s32[1,96]{1,0:T(1,128)} %bitcast.25, bf16[1536,128]{1,0:T(8,128)(2,1)} %refs_4_.1, ...), custom_call_target="tpu_custom_call" | custom-call | tf_op jit(solution)/shard_map/pallas_call | solution.py:858
  100.1 0.7 copy.27
  100.9 1.7 %copy.28 = f32[96,1,64,128]{3,2,1,0:T(8,128)} copy(f32[96,1,64,128]{3,2,1,0:T(8,128)S(1)} %bitcast.16) | data formatting | bytes 6291456
  102.6 1.7 %copy.29 = f32[96,1,64,128]{3,2,1,0:T(8,128)} copy(f32[96,1,64,128]{3,2,1,0:T(8,128)S(1)} %bitcast.15) | data formatting | bytes 6291456
